TPU v7x, 32 devices: a whole 2x2x4 slice. The times are simulated.
32 devices in a mesh: ep: 32 (over z, y, x, core).
Axes of the slice: x: 2, y: 2, z: 4, core: 2. Of those that a mesh axis runs over, the one named last changes fastest.
Arguments:
- tokens: bfloat16 [256, 2048], P('ep'), may hold values from -6 to 6
- premix_gain: float32 [2048], replicated, may hold values from 0.1 to 1.9
- postmix_gain: float32 [2048], replicated, may hold values from 0.1 to 1.9
- prefeed_gain: float32 [2048], replicated, may hold values from 0.1 to 1.9
- postfeed_gain: float32 [2048], replicated, may hold values from 0.1 to 1.9
- query_weight: bfloat16 [2048, 1024], P('ep'), may hold values from -0.125 to 0.125
- key_weight: bfloat16 [2048, 1024], P('ep'), may hold values from -0.125 to 0.125
- value_weight: bfloat16 [2048, 1024], P('ep'), may hold values from -0.125 to 0.125
- outgate_weight: bfloat16 [2048, 1024], P('ep'), may hold values from -0.125 to 0.125
- ingate_weight: bfloat16 [2048, 8], replicated, may hold values from -0.125 to 0.125
- forget_weight: bfloat16 [2048, 8], replicated, may hold values from -0.125 to 0.125
- ingate_bias: float32 [8], replicated, may hold values from -1 to 1
- forget_bias: float32 [8], replicated, may hold values from -1 to 5
- memory_state: float32 [256, 8, 128, 128], P('ep'), may hold values from -1.25 to 1.25
- normalizer: float32 [256, 8, 128], P('ep'), may hold values from -1.75 to 1.75
- stabilizer: float32 [256, 8], P('ep'), may hold values from -2 to 2
- output_weight: bfloat16 [1024, 2048], P(None, 'ep'), may hold values from -0.1875 to 0.1875
- expert_ids: int32 [256, 6], P('ep'), may hold values from 0 to 31, all different within a row; in each aligned block of 8 rows (0 to 7, 8 to 15, ...) at most 4 rows name the same one
- route_weights: float32 [256, 6], P('ep'), may hold values from 0.2 to 0.8
- expert_gate: bfloat16 [32, 2048, 512], P('ep'), may hold values from -0.125 to 0.125
- expert_up: bfloat16 [32, 2048, 512], P('ep'), may hold values from -0.125 to 0.125
- expert_down: bfloat16 [32, 512, 2048], P('ep'), may hold values from -0.25 to 0.25
- shared_gate: bfloat16 [2048, 512], replicated, may hold values from -0.125 to 0.125
- shared_up: bfloat16 [2048, 512], replicated, may hold values from -0.125 to 0.125
- shared_down: bfloat16 [512, 2048], replicated, may hold values from -0.25 to 0.25
Outputs:
- next_tokens: bfloat16 [256, 2048], P('ep')
- next_memory: float32 [256, 8, 128, 128], P('ep')
- next_normalizer: float32 [256, 8, 128], P('ep')
- next_stabilizer: float32 [256, 8], P('ep')
Inputs may be any that keep to these rules, and one draw needn't show every extreme that they name: `expert_ids`: each row names 6 different experts. Among the rows of one device no expert is named more than 4 times, and in every draw some expert is named exactly 4 times by the rows of some device.
All inputs are finite; a program needn't handle non-finite values.
Results may differ from a plain program's by a relative error of at most 0.0097.
Values may be sent and summed in bfloat16 or wider, within the bound.
A program may use at most 128 MiB of HBM per device.

v0:
```python
import jax
import jax.numpy as jnp
from jax import lax
from jax.sharding import PartitionSpec as P

epsilon = 1e-06


def rms_scale(values, gain_row):
    return (
        values * lax.rsqrt(jnp.mean(values * values, axis=-1, keepdims=True) + epsilon) * gain_row
    )


def rounded(values):
    return lax.optimization_barrier(values.astype(jnp.bfloat16))


def memory_step(
    queries,
    key_rows,
    value_rows,
    out_gate,
    input_pre,
    forget_pre,
    memory_state,
    normalizer,
    stabilizer,
):
    sequences = queries.shape[0]
    head_count = memory_state.shape[1]
    head_width = memory_state.shape[2]
    query_heads = queries.astype(jnp.float32).reshape(sequences, head_count, head_width)
    key_heads = key_rows.astype(jnp.float32).reshape(
        sequences, head_count, head_width
    ) * head_width ** (-0.5)
    value_heads = value_rows.astype(jnp.float32).reshape(sequences, head_count, head_width)
    carried = jax.nn.log_sigmoid(forget_pre) + stabilizer
    next_stabilizer = jnp.maximum(carried, input_pre)
    keep_old = jnp.exp(carried - next_stabilizer)
    write_new = jnp.exp(input_pre - next_stabilizer)
    local_score = write_new * jnp.sum(query_heads * key_heads, axis=-1)
    read_memory = jnp.einsum(
        "shvk,shk->shv", memory_state, query_heads, precision=lax.Precision.HIGHEST
    )
    numerator = keep_old[..., None] * read_memory + local_score[..., None] * value_heads
    denominator = keep_old * jnp.sum(normalizer * query_heads, axis=-1) + local_score
    memory_read = numerator / jnp.maximum(jnp.abs(denominator), 1.0)[..., None]
    gated_out = (
        jax.nn.sigmoid(out_gate.astype(jnp.float32))
        * memory_read.reshape(sequences, head_count * head_width)
    ).astype(jnp.bfloat16)
    next_memory = (
        keep_old[..., None, None] * memory_state
        + write_new[..., None, None] * value_heads[..., :, None] * key_heads[..., None, :]
    )
    next_normalizer = keep_old[..., None] * normalizer + write_new[..., None] * key_heads
    return (gated_out, next_memory, next_normalizer, next_stabilizer)


def expert_rows(row_block, gate_weight, up_weight, down_weight):
    gate_values = jnp.dot(row_block, gate_weight, preferred_element_type=jnp.float32)
    up_values = jnp.dot(row_block, up_weight, preferred_element_type=jnp.float32)
    inner_rows = (jax.nn.silu(gate_values) * up_values).astype(jnp.bfloat16)
    return jnp.dot(inner_rows, down_weight, preferred_element_type=jnp.float32)


def on_device(
    tokens,
    premix_gain,
    postmix_gain,
    prefeed_gain,
    postfeed_gain,
    query_weight,
    key_weight,
    value_weight,
    outgate_weight,
    ingate_weight,
    forget_weight,
    ingate_bias,
    forget_bias,
    memory_state,
    normalizer,
    stabilizer,
    output_weight,
    expert_ids,
    route_weights,
    expert_gate,
    expert_up,
    expert_down,
    shared_gate,
    shared_up,
    shared_down,
):
    sequences = tokens.shape[0]
    model_width = tokens.shape[1]
    memory_width = query_weight.shape[1]
    devices = lax.axis_size("ep")
    residual = tokens.astype(jnp.float32)
    normed = rms_scale(residual, premix_gain).astype(jnp.bfloat16)
    columns = (
        lax.all_to_all(query_weight, "ep", split_axis=1, concat_axis=0, tiled=True),
        lax.all_to_all(key_weight, "ep", split_axis=1, concat_axis=0, tiled=True),
        lax.all_to_all(value_weight, "ep", split_axis=1, concat_axis=0, tiled=True),
        lax.all_to_all(outgate_weight, "ep", split_axis=1, concat_axis=0, tiled=True),
    )
    stacked = jnp.concatenate(columns, axis=1)
    column_width = memory_width // devices
    piece_rows = lax.all_gather(normed, "ep", axis=0, tiled=True)
    product = jnp.dot(piece_rows, stacked, preferred_element_type=jnp.float32).astype(jnp.bfloat16)
    gathered = product.reshape(piece_rows.shape[0], 4, column_width)
    projected = lax.all_to_all(gathered, "ep", split_axis=0, concat_axis=2, tiled=True)
    input_pre = jnp.dot(normed, ingate_weight, preferred_element_type=jnp.float32) + ingate_bias
    forget_pre = jnp.dot(normed, forget_weight, preferred_element_type=jnp.float32) + forget_bias
    gated_out, next_memory, next_normalizer, next_stabilizer = memory_step(
        projected[:, 0],
        projected[:, 1],
        projected[:, 2],
        projected[:, 3],
        input_pre,
        forget_pre,
        memory_state,
        normalizer,
        stabilizer,
    )
    mixed_cols = jnp.dot(
        lax.all_gather(gated_out, "ep", axis=0, tiled=True),
        output_weight,
        preferred_element_type=jnp.float32,
    ).astype(jnp.bfloat16)
    mixed = lax.all_to_all(mixed_cols, "ep", split_axis=0, concat_axis=1, tiled=True)
    after_mix = rounded(residual + rms_scale(mixed.astype(jnp.float32), postmix_gain))
    after_float = after_mix.astype(jnp.float32)
    expert_input = rms_scale(after_float, prefeed_gain).astype(jnp.bfloat16)
    local_count = expert_gate.shape[0]
    experts_total = local_count * devices
    choose_count = expert_ids.shape[1]
    capacity = min(
        sequences, max(2, 2 * ((sequences * choose_count + experts_total - 1) // experts_total))
    )
    flat_ids = expert_ids.reshape(-1)
    one_hot = (flat_ids[:, None] == jnp.arange(experts_total, dtype=jnp.int32)[None, :]).astype(
        jnp.int32
    )
    earlier = jnp.cumsum(one_hot, axis=0) - one_hot
    slot_ids = jnp.sum(earlier * one_hot, axis=1)
    target = flat_ids * capacity + slot_ids
    pair_hot = (
        target[:, None] == jnp.arange(experts_total * capacity, dtype=jnp.int32)[None, :]
    ).astype(jnp.bfloat16)
    pair_rows = jnp.repeat(expert_input, choose_count, axis=0)
    outgoing = jnp.dot(pair_hot.T, pair_rows, preferred_element_type=jnp.float32).astype(
        jnp.bfloat16
    )
    outgoing = outgoing.reshape(experts_total, capacity, model_width)
    arrived = lax.all_to_all(outgoing, "ep", split_axis=0, concat_axis=0, tiled=True)
    item_count = arrived.shape[1]
    grouped = arrived.reshape(devices, local_count, item_count, model_width)
    gate_values = jnp.einsum(
        "nlid,ldf->nlif", grouped, expert_gate, preferred_element_type=jnp.float32
    )
    up_values = jnp.einsum("nlid,ldf->nlif", grouped, expert_up, preferred_element_type=jnp.float32)
    inner_rows = (jax.nn.silu(gate_values) * up_values).astype(jnp.bfloat16)
    answer = jnp.einsum(
        "nlif,lfd->nlid", inner_rows, expert_down, preferred_element_type=jnp.float32
    ).astype(jnp.bfloat16)
    answered = answer.reshape(devices * local_count, item_count, model_width)
    returned = lax.all_to_all(answered, "ep", split_axis=0, concat_axis=0, tiled=True)
    picked = jnp.dot(
        pair_hot,
        returned.reshape(experts_total * capacity, model_width),
        preferred_element_type=jnp.float32,
    )
    routed = jnp.sum(
        picked.reshape(sequences, choose_count, model_width) * route_weights[:, :, None], axis=1
    )
    shared_out = expert_rows(expert_input, shared_gate, shared_up, shared_down)
    next_tokens = (after_float + rms_scale(routed + shared_out, postfeed_gain)).astype(jnp.bfloat16)
    return (next_tokens, next_memory, next_normalizer, next_stabilizer)


def solution(mesh):
    in_specs = (
        P("ep", None),
        P(),
        P(),
        P(),
        P(),
        P("ep", None),
        P("ep", None),
        P("ep", None),
        P("ep", None),
        P(),
        P(),
        P(),
        P(),
        P("ep", None, None, None),
        P("ep", None, None),
        P("ep", None),
        P(None, "ep"),
        P("ep", None),
        P("ep", None),
        P("ep", None, None),
        P("ep", None, None),
        P("ep", None, None),
        P(),
        P(),
        P(),
    )
    out_specs = (P("ep", None), P("ep", None, None, None), P("ep", None, None), P("ep", None))
    return jax.shard_map(
        on_device, mesh=mesh, in_specs=in_specs, out_specs=out_specs, check_vma=False
    )
```

profile of v0, /device:TPU:0, one launch (start us, length us, event | category | flops | bytes accessed | tf_op | source)
XLA Modules:
  0.0 195.0 jit_solution(7154558388813392408)
XLA Ops:
  7.3 1.0 fusion.42
  8.3 1.5 fusion.44
  9.8 1.1 copy.71
  10.9 0.9 reshape.205
  11.8 7.3 %all-to-all-start = ((bf16[32,2,1024]{2,1,0:T(2,128)(2,1)}), bf16[32,2,1024]{2,1,0:T(2,128)(2,1)S(1)}, u32[]{:S(2)}, u32[]{:S(2)}) async-start(bf16[32,2,1024]{2,1,0:T(2,128)(2,1)} %reshape.205), calls=%async_computation | async-start | bytes 262144 | tf_op jit(solution)/shard_map/all_to_all | solution.py:102
  19.1 1.1 copy.73
  20.2 0.9 reshape.203
  21.0 6.3 %all-to-all-done = bf16[32,2,1024]{2,1,0:T(2,128)(2,1)S(1)} async-done(((bf16[32,2,1024]{2,1,0:T(2,128)(2,1)}), bf16[32,2,1024]{2,1,0:T(2,128)(2,1)S(1)}, u32[]{:S(2)}, u32[]{:S(2)}) %all-to-all-start) | async-done | bytes 131104 | tf_op jit(solution)/shard_map/all_to_all | solution.py:102
  27.3 2.6 %all-to-all-start.1 = ((bf16[32,2,1024]{2,1,0:T(2,128)(2,1)}), bf16[32,2,1024]{2,1,0:T(2,128)(2,1)S(1)}, u32[]{:S(2)}, u32[]{:S(2)}) async-start(bf16[32,2,1024]{2,1,0:T(2,128)(2,1)} %reshape.203), calls=%async_computation.1 | async-start | bytes 262144 | tf_op jit(solution)/shard_map/all_to_all | solution.py:103
  29.9 0.2 copy.75
  30.1 0.9 reshape.201
  31.0 0.1 fusion.72
  31.1 7.0 %all-to-all-done.1 = bf16[32,2,1024]{2,1,0:T(2,128)(2,1)S(1)} async-done(((bf16[32,2,1024]{2,1,0:T(2,128)(2,1)}), bf16[32,2,1024]{2,1,0:T(2,128)(2,1)S(1)}, u32[]{:S(2)}, u32[]{:S(2)}) %all-to-all-start.1) | async-done | bytes 131104 | tf_op jit(solution)/shard_map/all_to_all | solution.py:103
  38.1 2.6 %all-to-all-start.2 = ((bf16[32,2,1024]{2,1,0:T(2,128)(2,1)}), bf16[32,2,1024]{2,1,0:T(2,128)(2,1)S(1)}, u32[]{:S(2)}, u32[]{:S(2)}) async-start(bf16[32,2,1024]{2,1,0:T(2,128)(2,1)} %reshape.201), calls=%async_computation.2 | async-start | bytes 262144 | tf_op jit(solution)/shard_map/all_to_all | solution.py:104
  40.7 0.1 broadcast_multiply_fusion.1
  41.0 0.2 copy.77
  41.2 0.9 reshape.199
  42.0 0.2 reshape.206
  42.2 0.2 reshape.204
  42.5 6.7 %all-to-all-done.2 = bf16[32,2,1024]{2,1,0:T(2,128)(2,1)S(1)} async-done(((bf16[32,2,1024]{2,1,0:T(2,128)(2,1)}), bf16[32,2,1024]{2,1,0:T(2,128)(2,1)S(1)}, u32[]{:S(2)}, u32[]{:S(2)}) %all-to-all-start.2) | async-done | bytes 131104 | tf_op jit(solution)/shard_map/all_to_all | solution.py:104
  49.2 2.6 %all-to-all-start.3 = ((bf16[32,2,1024]{2,1,0:T(2,128)(2,1)}), bf16[32,2,1024]{2,1,0:T(2,128)(2,1)S(1)}, u32[]{:S(2)}, u32[]{:S(2)}) async-start(bf16[32,2,1024]{2,1,0:T(2,128)(2,1)} %reshape.199), calls=%async_computation.3 | async-start | bytes 262144 | tf_op jit(solution)/shard_map/all_to_all | solution.py:105
  51.9 0.3 all_to_all.88
  52.2 0.1 copy.74
  52.3 0.3 all_to_all.92
  52.6 0.2 reshape.202
  53.0 0.3 all_to_all.96
  53.2 6.8 %all-to-all-done.3 = bf16[32,2,1024]{2,1,0:T(2,128)(2,1)S(1)} async-done(((bf16[32,2,1024]{2,1,0:T(2,128)(2,1)}), bf16[32,2,1024]{2,1,0:T(2,128)(2,1)S(1)}, u32[]{:S(2)}, u32[]{:S(2)}) %all-to-all-start.3) | async-done | bytes 131104 | tf_op jit(solution)/shard_map/all_to_all | solution.py:105
  60.1 0.2 reshape.200
  60.4 0.3 all_to_all.100
  60.7 7.7 %all-gather.2.cloned.1.call-done = bf16[256,2048]{1,0:T(8,128)(2,1)} async-done(((bf16[8,2048]{1,0:T(8,128)(2,1)}), bf16[256,2048]{1,0:T(8,128)(2,1)}) %all-gather.2.cloned.1.call-update) | async-done | bytes 1048592 | tf_op jit(solution)/shard_map/all_gather | solution.py:109
  68.4 1.7 convolution_convert_fusion.2
  70.1 0.2 copy.79
  70.3 0.9 reshape.207
  71.1 3.5 %all-to-all-start.4 = ((bf16[32,2,512]{2,1,0:T(2,128)(2,1)}), bf16[32,2,512]{2,1,0:T(2,128)(2,1)S(1)}, u32[]{:S(2)}, u32[]{:S(2)}) async-start(bf16[32,2,512]{2,1,0:T(2,128)(2,1)} %reshape.207), calls=%async_computation.4 | async-start | bytes 131072 | tf_op jit(solution)/shard_map/all_to_all | solution.py:112
  74.8 0.2 select_reduce_fusion
  75.0 7.1 %all-to-all-done.4 = bf16[32,2,512]{2,1,0:T(2,128)(2,1)S(1)} async-done(((bf16[32,2,512]{2,1,0:T(2,128)(2,1)}), bf16[32,2,512]{2,1,0:T(2,128)(2,1)S(1)}, u32[]{:S(2)}, u32[]{:S(2)}) %all-to-all-start.4) | async-done | bytes 65568 | tf_op jit(solution)/shard_map/all_to_all | solution.py:112
  82.1 0.2 reshape.208
  82.4 0.3 all_to_all.104
  82.7 5.6 %fusion.53 = f32[8,8,1,128]{3,2,1,0:T(1,128)S(1)} fusion(f32[8,8,128,128]{3,2,1,0:T(8,128)} %param.38, bf16[8,8,128,1]{2,0,1,3:T(8,128)(2,1)S(1)} %get-tuple-element.13), kind=kOutput, calls=%fused_computation.63 | convolution fusion | flops 12582912 | bytes 4243456 | tf_op jit(solution)/shard_map/shvk,shk->shv/dot_general | solution.py:43
  88.4 0.7 multiply_add_fusion.1
  89.2 38.7 %all_gather.7 = bf16[256,1024]{1,0:T(8,128)(2,1)S(1)} all-gather(bf16[8,1024]{1,0:T(8,128)(2,1)S(1)} %fusion.52), channel_id=1, replica_groups=mesh['ep'=32] {'ep'}, dimensions={0}, use_global_device_ids=true | all-gather | bytes 540672 | tf_op jit(solution)/shard_map/all_gather | solution.py:127
  127.9 0.3 convolution_convert_fusion.3
  128.2 0.1 copy.85
  128.3 0.7 reshape.209
  129.0 2.6 %all-to-all-start.5 = ((bf16[32,2,256]{2,1,0:T(2,128)(2,1)}), bf16[32,2,256]{2,1,0:T(2,128)(2,1)S(1)}, u32[]{:S(2)}, u32[]{:S(2)}) async-start(bf16[32,2,256]{2,1,0:T(2,128)(2,1)} %reshape.209), calls=%async_computation.5 | async-start | bytes 65536 | tf_op jit(solution)/shard_map/all_to_all | solution.py:131
  131.6 7.2 %all-to-all-done.5 = bf16[32,2,256]{2,1,0:T(2,128)(2,1)S(1)} async-done(((bf16[32,2,256]{2,1,0:T(2,128)(2,1)}), bf16[32,2,256]{2,1,0:T(2,128)(2,1)S(1)}, u32[]{:S(2)}, u32[]{:S(2)}) %all-to-all-start.5) | async-done | bytes 32800 | tf_op jit(solution)/shard_map/all_to_all | solution.py:131
  138.9 0.1 reshape.210
  139.0 0.1 fusion.40
  139.4 0.1 fusion.46
  139.7 0.4 convolution_convert_fusion.1
  140.1 1.0 reshape.181
  141.1 2.8 %all-to-all-start.6 = ((bf16[32,4,2048]{2,1,0:T(4,128)(2,1)}), bf16[32,4,2048]{2,1,0:T(4,128)(2,1)S(1)}, u32[]{:S(2)}, u32[]{:S(2)}) async-start(bf16[32,4,2048]{2,1,0:T(4,128)(2,1)} %reshape.181), calls=%async_computation.6 | async-start | bytes 1048576 | tf_op jit(solution)/shard_map/all_to_all | solution.py:156
  144.0 15.4 %all-to-all-done.6 = bf16[32,4,2048]{2,1,0:T(4,128)(2,1)S(1)} async-done(((bf16[32,4,2048]{2,1,0:T(4,128)(2,1)}), bf16[32,4,2048]{2,1,0:T(4,128)(2,1)S(1)}, u32[]{:S(2)}, u32[]{:S(2)}) %all-to-all-start.6) | async-done | bytes 524320 | tf_op jit(solution)/shard_map/all_to_all | solution.py:156
  159.4 2.2 %fusion.5 = f32[32,1,4,512]{3,0,2,1:T(8,128)S(1)} fusion(bf16[1,2048,512]{2,1,0:T(8,128)(2,1)} %param.44, bf16[32,4,2048]{2,1,0:T(4,128)(2,1)S(1)} %all-to-all-done.6), kind=kOutput, calls=%fused_computation.10 | convolution fusion | flops 268435456 | bytes 2883584 | tf_op jit(solution)/shard_map/nlid,ldf->nlif/dot_general | solution.py:159
  161.6 2.6 %convolution_convert_fusion = bf16[32,4,2048]{2,0,1:T(8,128)(2,1)S(1)} fusion(bf16[1,512,2048]{2,1,0:T(8,128)(2,1)S(1)} %copy-done, bf16[1,2048,512]{2,1,0:T(8,128)(2,1)} %param.45, bf16[32,4,2048]{2,1,0:T(4,128)(2,1)S(1)} %all-to-all-done.6, f32[32,1,4,512]{3,0,2,1:T(8,128)S(1)} %fusion.5), kind=kOutput, calls=%fused_computation.1 | convolution fusion | flops 537526272 | bytes 5505024 | tf_op jit(solution)/shard_map/nlif,lfd->nlid/dot_general | solution.py:164
  164.3 1.2 copy.90
  165.5 2.9 %all-to-all-start.7 = ((bf16[32,4,2048]{2,1,0:T(4,128)(2,1)}), bf16[32,4,2048]{2,1,0:T(4,128)(2,1)S(1)}, u32[]{:S(2)}, u32[]{:S(2)}) async-start(bf16[32,4,2048]{2,1,0:T(4,128)(2,1)} %copy.90), calls=%async_computation.7 | async-start | bytes 1048576 | tf_op jit(solution)/shard_map/all_to_all | solution.py:168
  168.7 4.5 %multiply_add_fusion = f32[8,8,128,128]{3,2,1,0:T(8,128)} fusion(f32[8,8,128,128]{3,2,1,0:T(8,128)} %param.38, f32[8,8,128]{2,1,0:T(8,128)S(1)} %copy-done.4, f32[8,8,128]{2,1,0:T(8,128)S(1)} %copy.93, f32[8,8]{1,0:T(8,128)S(1)} %get-tuple-element.10), kind=kLoop, calls=%fused_computation | loop fusion | flops 3145728 | bytes 8454400 | tf_op jit(solution)/shard_map/add | solution.py:54
  173.2 0.4 fusion.76
  173.6 10.4 %all-to-all-done.7 = bf16[32,4,2048]{2,1,0:T(4,128)(2,1)S(1)} async-done(((bf16[32,4,2048]{2,1,0:T(4,128)(2,1)}), bf16[32,4,2048]{2,1,0:T(4,128)(2,1)S(1)}, u32[]{:S(2)}, u32[]{:S(2)}) %all-to-all-start.7) | async-done | bytes 524320 | tf_op jit(solution)/shard_map/all_to_all | solution.py:168
  184.0 0.1 reshape.197
  184.1 0.3 fusion.11
  184.4 3.1 %multiply_reduce_fusion = (f32[8]{0:T(128)S(1)}, f32[8,2048]{1,0:T(8,128)S(1)}) fusion(f32[8,2048]{1,0:T(8,128)S(1)} %fusion.11, bf16[512,2048]{1,0:T(8,128)(2,1)} %param.49, bf16[8,2048]{1,0:T(8,128)(2,1)S(1)} %fusion.48, bf16[2048,512]{1,0:T(8,128)(2,1)} %param.48, f32[8,512]{1,0:T(8,128)S(1)} %fusion.76), kind=kOutput, calls=%fused_computation.56 | convolution fusion | flops 33628152 | bytes 4374560 | tf_op jit(solution)/shard_map/dot_general | solution.py:65
  187.5 0.7 fusion.49
  (77 shorter events, 1.8 us)
Async XLA Ops:
  7.2 154.4 %copy-start = (bf16[1,512,2048]{2,1,0:T(8,128)(2,1)S(1)}, bf16[1,512,2048]{2,1,0:T(8,128)(2,1)}, u32[]{:S(2)}) copy-start(bf16[1,512,2048]{2,1,0:T(8,128)(2,1)} %param.46) | copy-start | bytes 6291460
  7.2 22.7 %copy-start.5 = (bf16[64,1024]{1,0:T(8,128)(2,1)S(1)}, bf16[64,1024]{1,0:T(8,128)(2,1)}, u32[]{:S(2)}) copy-start(bf16[64,1024]{1,0:T(8,128)(2,1)} %param.32) | copy-start | bytes 393220
  7.2 23.8 %copy-start.16 = (f32[8,8]{1,0:T(8,128)S(1)}, f32[8,8]{1,0:T(8,128)}, u32[]{:S(2)}) copy-start(f32[8,8]{1,0:T(8,128)} %param.40) | copy-start | bytes 772
  7.2 23.7 %copy-start.18 = (f32[8]{0:T(128)S(1)}, f32[8]{0:T(128)}, u32[]{:S(2)}) copy-start(f32[8]{0:T(128)} %param.37) | copy-start | bytes 100
  7.2 23.7 %copy-start.9 = (bf16[2048,8]{0,1:T(8,128)(2,1)S(1)}, bf16[2048,8]{0,1:T(8,128)(2,1)}, u32[]{:S(2)}) copy-start(bf16[2048,8]{0,1:T(8,128)(2,1)} %param.35) | copy-start | bytes 98308
  7.2 33.5 %copy-start.19 = (f32[8]{0:T(128)S(1)}, f32[8]{0:T(128)}, u32[]{:S(2)}) copy-start(f32[8]{0:T(128)} %param.36) | copy-start | bytes 100
  7.2 33.5 %copy-start.10 = (bf16[2048,8]{0,1:T(8,128)(2,1)S(1)}, bf16[2048,8]{0,1:T(8,128)(2,1)}, u32[]{:S(2)}) copy-start(bf16[2048,8]{0,1:T(8,128)(2,1)} %param.34) | copy-start | bytes 98308
  7.2 33.6 %copy-start.11 = (s32[8,6]{1,0:T(8,128)S(1)}, s32[8,6]{1,0:T(8,128)}, u32[]{:S(2)}) copy-start(s32[8,6]{1,0:T(8,128)} %param.42) | copy-start | bytes 580
  7.3 33.7 %copy-start.6 = (bf16[64,1024]{1,0:T(8,128)(2,1)S(1)}, bf16[64,1024]{1,0:T(8,128)(2,1)}, u32[]{:S(2)}) copy-start(bf16[64,1024]{1,0:T(8,128)(2,1)} %param.33) | copy-start | bytes 393220
  7.3 61.1 %all-gather.2.cloned.1.call-start = ((), (), s32[]{:S(2)}) async-start(), calls=%async_computation.8 | async-start | bytes 1081344 | tf_op jit(solution)/shard_map/all_gather | solution.py:109
  9.8 21.1 %copy-start.2 = (bf16[8,2048]{1,0:T(8,128)(2,1)S(1)}, bf16[8,2048]{1,0:T(8,128)(2,1)}, u32[]{:S(2)}) copy-start(bf16[8,2048]{1,0:T(8,128)(2,1)} %fusion.44) | copy-start | bytes 98308
  11.8 15.5 %all-to-all-start = ((bf16[32,2,1024]{2,1,0:T(2,128)(2,1)}), bf16[32,2,1024]{2,1,0:T(2,128)(2,1)S(1)}, u32[]{:S(2)}, u32[]{:S(2)}) async-start(bf16[32,2,1024]{2,1,0:T(2,128)(2,1)} %reshape.205), calls=%async_computation | async-start | bytes 262144 | tf_op jit(solution)/shard_map/all_to_all | solution.py:102
  27.3 10.8 %all-to-all-start.1 = ((bf16[32,2,1024]{2,1,0:T(2,128)(2,1)}), bf16[32,2,1024]{2,1,0:T(2,128)(2,1)S(1)}, u32[]{:S(2)}, u32[]{:S(2)}) async-start(bf16[32,2,1024]{2,1,0:T(2,128)(2,1)} %reshape.203), calls=%async_computation.1 | async-start | bytes 262144 | tf_op jit(solution)/shard_map/all_to_all | solution.py:103
  38.1 11.1 %all-to-all-start.2 = ((bf16[32,2,1024]{2,1,0:T(2,128)(2,1)}), bf16[32,2,1024]{2,1,0:T(2,128)(2,1)S(1)}, u32[]{:S(2)}, u32[]{:S(2)}) async-start(bf16[32,2,1024]{2,1,0:T(2,128)(2,1)} %reshape.201), calls=%async_computation.2 | async-start | bytes 262144 | tf_op jit(solution)/shard_map/all_to_all | solution.py:104
  40.9 47.5 %copy-start.12 = (f32[8,8]{1,0:T(8,128)}, f32[8,8]{1,0:T(8,128)S(1)}, u32[]{:S(2)}) copy-start(f32[8,8]{1,0:T(8,128)S(1)} %get-tuple-element.8) | copy-start | bytes 772
  49.2 10.8 %all-to-all-start.3 = ((bf16[32,2,1024]{2,1,0:T(2,128)(2,1)}), bf16[32,2,1024]{2,1,0:T(2,128)(2,1)S(1)}, u32[]{:S(2)}, u32[]{:S(2)}) async-start(bf16[32,2,1024]{2,1,0:T(2,128)(2,1)} %reshape.199), calls=%async_computation.3 | async-start | bytes 262144 | tf_op jit(solution)/shard_map/all_to_all | solution.py:105
  71.1 11.0 %all-to-all-start.4 = ((bf16[32,2,512]{2,1,0:T(2,128)(2,1)}), bf16[32,2,512]{2,1,0:T(2,128)(2,1)S(1)}, u32[]{:S(2)}, u32[]{:S(2)}) async-start(bf16[32,2,512]{2,1,0:T(2,128)(2,1)} %reshape.207), calls=%async_computation.4 | async-start | bytes 131072 | tf_op jit(solution)/shard_map/all_to_all | solution.py:112
  82.7 5.6 %copy-start.7 = (f32[8,8,128]{2,1,0:T(8,128)S(1)}, f32[8,8,128]{2,1,0:T(8,128)}, u32[]{:S(2)}) copy-start(f32[8,8,128]{2,1,0:T(8,128)} %param.39) | copy-start | bytes 98308
  82.7 45.2 %copy-start.8 = (bf16[1024,64]{0,1:T(8,128)(2,1)S(1)}, bf16[1024,64]{0,1:T(8,128)(2,1)}, u32[]{:S(2)}) copy-start(bf16[1024,64]{0,1:T(8,128)(2,1)} %param.41) | copy-start | bytes 393220
  88.3 51.0 %copy-start.3 = (bf16[8,2048]{1,0:T(8,128)(2,1)S(1)}, bf16[8,2048]{1,0:T(8,128)(2,1)}, u32[]{:S(2)}) copy-start(bf16[8,2048]{1,0:T(8,128)(2,1)} %param.25) | copy-start | bytes 98308
  88.3 51.0 %copy-start.13 = (f32[2048]{0:T(1024)S(1)}, f32[2048]{0:T(1024)}, u32[]{:S(2)}) copy-start(f32[2048]{0:T(1024)} %param.27) | copy-start | bytes 24580
  88.3 51.2 %copy-start.14 = (f32[2048]{0:T(1024)S(1)}, f32[2048]{0:T(1024)}, u32[]{:S(2)}) copy-start(f32[2048]{0:T(1024)} %param.28) | copy-start | bytes 24580
  129.0 9.8 %all-to-all-start.5 = ((bf16[32,2,256]{2,1,0:T(2,128)(2,1)}), bf16[32,2,256]{2,1,0:T(2,128)(2,1)S(1)}, u32[]{:S(2)}, u32[]{:S(2)}) async-start(bf16[32,2,256]{2,1,0:T(2,128)(2,1)} %reshape.209), calls=%async_computation.5 | async-start | bytes 65536 | tf_op jit(solution)/shard_map/all_to_all | solution.py:131
  141.1 18.2 %all-to-all-start.6 = ((bf16[32,4,2048]{2,1,0:T(4,128)(2,1)}), bf16[32,4,2048]{2,1,0:T(4,128)(2,1)S(1)}, u32[]{:S(2)}, u32[]{:S(2)}) async-start(bf16[32,4,2048]{2,1,0:T(4,128)(2,1)} %reshape.181), calls=%async_computation.6 | async-start | bytes 1048576 | tf_op jit(solution)/shard_map/all_to_all | solution.py:156
  164.2 4.2 %copy-start.17 = (f32[8,6]{1,0:T(8,128)S(1)}, f32[8,6]{1,0:T(8,128)}, u32[]{:S(2)}) copy-start(f32[8,6]{1,0:T(8,128)} %param.43) | copy-start | bytes 580
  164.3 4.5 %copy-start.4 = (f32[8,8,128]{2,1,0:T(8,128)S(1)}, f32[8,8,128]{2,1,0:T(8,128)}, u32[]{:S(2)}) copy-start(f32[8,8,128]{2,1,0:T(8,128)} %get-tuple-element.17) | copy-start | bytes 98308
  165.5 18.5 %all-to-all-start.7 = ((bf16[32,4,2048]{2,1,0:T(4,128)(2,1)}), bf16[32,4,2048]{2,1,0:T(4,128)(2,1)S(1)}, u32[]{:S(2)}, u32[]{:S(2)}) async-start(bf16[32,4,2048]{2,1,0:T(4,128)(2,1)} %copy.90), calls=%async_computation.7 | async-start | bytes 1048576 | tf_op jit(solution)/shard_map/all_to_all | solution.py:168
  168.7 4.5 %copy-start.1 = (bf16[2048,512]{1,0:T(8,128)(2,1)S(1)}, bf16[2048,512]{1,0:T(8,128)(2,1)}, u32[]{:S(2)}) copy-start(bf16[2048,512]{1,0:T(8,128)(2,1)} %param.47) | copy-start | bytes 6291460
  184.4 3.1 %copy-start.15 = (f32[2048]{0:T(1024)S(1)}, f32[2048]{0:T(1024)}, u32[]{:S(2)}) copy-start(f32[2048]{0:T(1024)} %param.29) | copy-start | bytes 24580
Sparse Core Ops, SparseCore 0:
  11.5 56.8 all-gather.1
where the time goes:
time: 196 us; the launch traced here: 195 us
  waiting for transfers between devices  74.7 us (38%)
  blocking collectives  38.7 us (20%)
  starting transfers between devices  26.9 us (14%)
  matrix products  16.8 us (9%)
  between operations  14.6 us (7%)
  local copies, waits for them, and re-layouts  14 us (7%)
  other arithmetic  9.39 us (5%)
    all_gather x1, blocking collectives, on_device(): lax.all_gather(gated_out, 'ep', axis=0, tiled=True)  38.7 us
    all_to_all x1, waiting for transfers between devices, on_device(): lax.all_to_all(outgoing, 'ep', split_axis=0, concat_axis=0, tiled=True)  15.4 us
    all_to_all x1, waiting for transfers between devices, on_device(): lax.all_to_all(answered, 'ep', split_axis=0, concat_axis=0, tiled=True)  10.4 us
    unnamed x57, local copies, waits for them, and re-layouts  8.88 us
    all_gather x1, waiting for transfers between devices, on_device(): piece_rows = lax.all_gather(normed, 'ep', axis=0, tiled=True)  7.7 us
    all_to_all x1, starting transfers between devices, on_device(): lax.all_to_all(query_weight, 'ep', split_axis=1, concat_axis=0, tiled=True)  7.33 us
    all_to_all x1, waiting for transfers between devices, on_device(): lax.all_to_all(mixed_cols, 'ep', split_axis=0, concat_axis=1, tiled=True)  7.24 us
    all_to_all x1, waiting for transfers between devices, on_device(): lax.all_to_all(gathered, 'ep', split_axis=0, concat_axis=2, tiled=True)  7.08 us
  transfers between devices with their start and end apart: 9, of which 9 were waited for; matrix products, arithmetic and copies ran while one was open for 7% of the time, Pallas kernels for 0%

commit v1 on v0

v1 whole, which is shorter than its diff:
```python
import functools

import jax
import jax.numpy as jnp
from jax import lax
from jax.experimental import pallas as pl
from jax.experimental.pallas import tpu as pltpu
from jax.sharding import PartitionSpec as P

epsilon = 1e-06
LANES = 128
MESH = pl.DeviceIdType.MESH
VM = pl.BlockSpec(memory_space=pltpu.VMEM)
ANY = pl.BlockSpec(memory_space=pl.ANY)


def rms_scale(values, gain_row):
    return (
        values * lax.rsqrt(jnp.mean(values * values, axis=-1, keepdims=True) + epsilon) * gain_row
    )


def rounded(values):
    return lax.optimization_barrier(values.astype(jnp.bfloat16))


def greet(n, me):
    sem = pltpu.get_barrier_semaphore()

    def signal(i, carry):
        pl.semaphore_signal(
            sem, inc=1, device_id=(lax.rem(me + i, n),), device_id_type=MESH
        )
        return carry

    lax.fori_loop(1, n, signal, 0)


def greeted(n):
    pl.semaphore_wait(pltpu.get_barrier_semaphore(), n - 1)


def send(src, dst, send_sem, recv_sem, peer):
    pltpu.make_async_remote_copy(
        src_ref=src,
        dst_ref=dst,
        send_sem=send_sem,
        recv_sem=recv_sem,
        device_id=(peer,),
        device_id_type=MESH,
    ).start()


def drain(ref, sem):
    pltpu.make_async_copy(ref, ref, sem).wait()


def project_kernel(
    n,
    groups,
    normed_ref,
    query_ref,
    key_ref,
    value_ref,
    gate_ref,
    out_ref,
    rows_buf,
    weight_buf,
    product_buf,
    result_buf,
    send_sems,
    recv_sems,
):
    me = lax.axis_index("ep")
    blocks = n // groups
    per_matrix = blocks // 4
    mine, turn = me // groups, lax.rem(me, groups)
    greet(n, me)
    weights = (query_ref, key_ref, value_ref, gate_ref)

    def column(block):
        return pl.ds(pl.multiple_of(lax.rem(block, per_matrix) * LANES, LANES), LANES)

    for index, ref in enumerate(weights):

        @pl.when(mine // per_matrix == index)
        def _():
            pltpu.make_async_copy(
                ref.at[:, column(mine)], weight_buf.at[me], recv_sems.at[1]
            ).start()

    pltpu.make_async_copy(normed_ref, rows_buf.at[mine], recv_sems.at[0]).start()
    greeted(n)

    def send_rows(i, carry):
        place = lax.rem(mine + i, blocks)
        send(
            normed_ref,
            rows_buf.at[mine],
            send_sems.at[0],
            recv_sems.at[0],
            place * groups + turn,
        )
        return carry

    def send_weights(i, carry):
        peer = lax.rem(me + i, n)
        block = peer // groups
        for index, ref in enumerate(weights):

            @pl.when(block // per_matrix == index)
            def _():
                send(
                    ref.at[:, column(block)],
                    weight_buf.at[me],
                    send_sems.at[1],
                    recv_sems.at[1],
                    peer,
                )

        return carry

    lax.fori_loop(1, n, send_weights, 0)
    lax.fori_loop(1, blocks, send_rows, 0)
    drain(rows_buf, recv_sems.at[0])
    drain(weight_buf, recv_sems.at[1])
    rows = rows_buf[...].reshape(rows_buf.shape[0] * rows_buf.shape[1], rows_buf.shape[2])
    weight = weight_buf[...].reshape(weight_buf.shape[0] * weight_buf.shape[1], LANES)
    product = jnp.dot(rows, weight, preferred_element_type=jnp.float32)
    product_buf[...] = product.reshape(product_buf.shape).astype(jnp.bfloat16)
    pltpu.make_async_copy(product_buf.at[mine], result_buf.at[mine], recv_sems.at[2]).start()

    def send_product(i, carry):
        place = lax.rem(mine + i, blocks)
        send(
            product_buf.at[place],
            result_buf.at[mine],
            send_sems.at[2],
            recv_sems.at[2],
            place * groups + turn,
        )
        return carry

    lax.fori_loop(1, blocks, send_product, 0)
    drain(result_buf, recv_sems.at[2])
    for block in range(blocks):
        out_ref[:, block * LANES : (block + 1) * LANES] = result_buf[block].astype(jnp.float32)
    drain(rows_buf.at[pl.ds(0, blocks - 1)], send_sems.at[0])
    drain(weight_buf.at[pl.ds(0, n - 1)], send_sems.at[1])
    drain(result_buf.at[pl.ds(0, blocks - 1)], send_sems.at[2])


def project(n, normed, *weights):
    sequences, width = normed.shape
    depth, columns = weights[0].shape
    blocks = 4 * columns // LANES
    groups = n // blocks
    return pl.pallas_call(
        functools.partial(project_kernel, n, groups),
        out_shape=jax.ShapeDtypeStruct((sequences, 4 * columns), jnp.float32),
        in_specs=[VM, ANY, ANY, ANY, ANY],
        out_specs=VM,
        scratch_shapes=[
            pltpu.VMEM((blocks, sequences, width), jnp.bfloat16),
            pltpu.VMEM((n, depth, LANES), jnp.bfloat16),
            pltpu.VMEM((blocks, sequences, LANES), jnp.bfloat16),
            pltpu.VMEM((blocks, sequences, LANES), jnp.bfloat16),
            pltpu.SemaphoreType.DMA((3,)),
            pltpu.SemaphoreType.DMA((3,)),
        ],
        compiler_params=pltpu.CompilerParams(collective_id=0, has_side_effects=True),
    )(normed, *weights)


def mix_kernel(
    n, gated_ref, weight_ref, out_ref, rows_buf, product_buf, result_buf, send_sems, recv_sems
):
    me = lax.axis_index("ep")
    greet(n, me)
    pltpu.make_async_copy(gated_ref, rows_buf.at[me], recv_sems.at[0]).start()
    greeted(n)

    def send_rows(i, carry):
        send(
            gated_ref, rows_buf.at[me], send_sems.at[0], recv_sems.at[0], lax.rem(me + i, n)
        )
        return carry

    lax.fori_loop(1, n, send_rows, 0)
    drain(rows_buf, recv_sems.at[0])
    rows = rows_buf[...].reshape(rows_buf.shape[0] * rows_buf.shape[1], rows_buf.shape[2])
    product = jnp.dot(rows, weight_ref[...], preferred_element_type=jnp.float32)
    product_buf[...] = product.reshape(product_buf.shape).astype(jnp.bfloat16)
    pltpu.make_async_copy(product_buf.at[me], result_buf.at[me], recv_sems.at[1]).start()

    def send_product(i, carry):
        peer = lax.rem(me + i, n)
        send(product_buf.at[peer], result_buf.at[me], send_sems.at[1], recv_sems.at[1], peer)
        return carry

    lax.fori_loop(1, n, send_product, 0)
    drain(result_buf, recv_sems.at[1])
    out_ref[...] = result_buf[...]
    drain(rows_buf.at[pl.ds(0, n - 1)], send_sems.at[0])
    drain(result_buf.at[pl.ds(0, n - 1)], send_sems.at[1])


def mix(n, gated, weight):
    sequences, width = gated.shape
    columns = weight.shape[1]
    return pl.pallas_call(
        functools.partial(mix_kernel, n),
        out_shape=jax.ShapeDtypeStruct((n, sequences, columns), jnp.bfloat16),
        in_specs=[VM, VM],
        out_specs=VM,
        scratch_shapes=[
            pltpu.VMEM((n, sequences, width), jnp.bfloat16),
            pltpu.VMEM((n, sequences, columns), jnp.bfloat16),
            pltpu.VMEM((n, sequences, columns), jnp.bfloat16),
            pltpu.SemaphoreType.DMA((2,)),
            pltpu.SemaphoreType.DMA((2,)),
        ],
        compiler_params=pltpu.CompilerParams(collective_id=1, has_side_effects=True),
    )(gated, weight)


def two_layer(rows, gate_weight, up_weight, down_weight):
    gate_values = jnp.dot(rows, gate_weight, preferred_element_type=jnp.float32)
    up_values = jnp.dot(rows, up_weight, preferred_element_type=jnp.float32)
    inner_rows = (gate_values * jax.nn.sigmoid(gate_values) * up_values).astype(jnp.bfloat16)
    return jnp.dot(inner_rows, down_weight, preferred_element_type=jnp.float32)


def expert_kernel(
    n,
    rows_ref,
    dispatch_ref,
    combine_ref,
    *refs,
):
    weights_hbm, out_ref = refs[:6], refs[6]
    weights, (outgoing, arrived, answer, returned, load_sems, send_sems, recv_sems) = (
        refs[7:13],
        refs[13:],
    )
    me = lax.axis_index("ep")
    greet(n, me)
    loads = [
        pltpu.make_async_copy(source, target, load_sems.at[index])
        for index, (source, target) in enumerate(zip(weights_hbm, weights))
    ]
    for index in (3, 4, 5, 0, 1, 2):
        loads[index].start()
    local, capacity = weights[0].shape[0], outgoing.shape[2]
    width = rows_ref.shape[1]
    outgoing[...] = jnp.dot(
        dispatch_ref[...], rows_ref[...], preferred_element_type=jnp.float32
    ).reshape(outgoing.shape).astype(jnp.bfloat16)
    pltpu.make_async_copy(outgoing.at[me], arrived.at[me], recv_sems.at[0]).start()
    greeted(n)

    def exchange(source, target, stage):
        def one(i, carry):
            peer = lax.rem(me + i, n)
            send(source.at[peer], target.at[me], send_sems.at[stage], recv_sems.at[stage], peer)
            return carry

        lax.fori_loop(1, n, one, 0)

    exchange(outgoing, arrived, 0)
    for index in (3, 4, 5):
        loads[index].wait()
    shared_out = two_layer(
        rows_ref[...], weights[3][...], weights[4][...], weights[5][...]
    )
    for index in (0, 1, 2):
        loads[index].wait()
    drain(arrived, recv_sems.at[0])
    for item in range(local):
        block = arrived[:, item].astype(jnp.float32).reshape(n * capacity, width)
        answer[:, item] = (
            two_layer(
                block.astype(jnp.bfloat16),
                weights[0][item],
                weights[1][item],
                weights[2][item],
            )
            .reshape(n, capacity, width)
            .astype(jnp.bfloat16)
        )
    pltpu.make_async_copy(answer.at[me], returned.at[me], recv_sems.at[1]).start()
    exchange(answer, returned, 1)
    combine = combine_ref[...]
    high = combine.astype(jnp.bfloat16)
    low = (combine - high.astype(jnp.float32)).astype(jnp.bfloat16)
    drain(returned, recv_sems.at[1])
    picked = (
        returned[...].astype(jnp.float32).reshape(combine.shape[1], width).astype(jnp.bfloat16)
    )
    out_ref[...] = (
        shared_out
        + jnp.dot(high, picked, preferred_element_type=jnp.float32)
        + jnp.dot(low, picked, preferred_element_type=jnp.float32)
    )
    drain(arrived.at[pl.ds(0, n - 1)], send_sems.at[0])
    drain(returned.at[pl.ds(0, n - 1)], send_sems.at[1])


def experts(n, rows, dispatch, combine, *weights):
    sequences, width = rows.shape
    local = weights[0].shape[0]
    capacity = dispatch.shape[0] // (n * local)
    slots = pltpu.VMEM((n, local, capacity, width), jnp.bfloat16)
    return pl.pallas_call(
        functools.partial(expert_kernel, n),
        out_shape=jax.ShapeDtypeStruct((sequences, width), jnp.float32),
        in_specs=[VM, VM, VM] + [ANY] * 6,
        out_specs=VM,
        scratch_shapes=[pltpu.VMEM(w.shape, w.dtype) for w in weights]
        + [slots] * 4
        + [
            pltpu.SemaphoreType.DMA((6,)),
            pltpu.SemaphoreType.DMA((2,)),
            pltpu.SemaphoreType.DMA((2,)),
        ],
        compiler_params=pltpu.CompilerParams(
            collective_id=2, has_side_effects=True, vmem_limit_bytes=50 * 1024 * 1024
        ),
    )(rows, dispatch, combine, *weights)


def memory_step(
    queries,
    key_rows,
    value_rows,
    out_gate,
    input_pre,
    forget_pre,
    memory_state,
    normalizer,
    stabilizer,
):
    sequences = queries.shape[0]
    head_count = memory_state.shape[1]
    head_width = memory_state.shape[2]
    query_heads = queries.astype(jnp.float32).reshape(sequences, head_count, head_width)
    key_heads = key_rows.astype(jnp.float32).reshape(
        sequences, head_count, head_width
    ) * head_width ** (-0.5)
    value_heads = value_rows.astype(jnp.float32).reshape(sequences, head_count, head_width)
    carried = jax.nn.log_sigmoid(forget_pre) + stabilizer
    next_stabilizer = jnp.maximum(carried, input_pre)
    keep_old = jnp.exp(carried - next_stabilizer)
    write_new = jnp.exp(input_pre - next_stabilizer)
    local_score = write_new * jnp.sum(query_heads * key_heads, axis=-1)
    read_memory = jnp.einsum(
        "shvk,shk->shv", memory_state, query_heads, precision=lax.Precision.HIGHEST
    )
    numerator = keep_old[..., None] * read_memory + local_score[..., None] * value_heads
    denominator = keep_old * jnp.sum(normalizer * query_heads, axis=-1) + local_score
    memory_read = numerator / jnp.maximum(jnp.abs(denominator), 1.0)[..., None]
    gated_out = (
        jax.nn.sigmoid(out_gate.astype(jnp.float32))
        * memory_read.reshape(sequences, head_count * head_width)
    ).astype(jnp.bfloat16)
    next_memory = (
        keep_old[..., None, None] * memory_state
        + write_new[..., None, None] * value_heads[..., :, None] * key_heads[..., None, :]
    )
    next_normalizer = keep_old[..., None] * normalizer + write_new[..., None] * key_heads
    return (gated_out, next_memory, next_normalizer, next_stabilizer)


def on_device(
    tokens,
    premix_gain,
    postmix_gain,
    prefeed_gain,
    postfeed_gain,
    query_weight,
    key_weight,
    value_weight,
    outgate_weight,
    ingate_weight,
    forget_weight,
    ingate_bias,
    forget_bias,
    memory_state,
    normalizer,
    stabilizer,
    output_weight,
    expert_ids,
    route_weights,
    expert_gate,
    expert_up,
    expert_down,
    shared_gate,
    shared_up,
    shared_down,
):
    sequences = tokens.shape[0]
    model_width = tokens.shape[1]
    memory_width = query_weight.shape[1]
    devices = lax.axis_size("ep")
    residual = tokens.astype(jnp.float32)
    normed = rms_scale(residual, premix_gain).astype(jnp.bfloat16)
    projected = project(devices, normed, query_weight, key_weight, value_weight, outgate_weight)
    projected = projected.reshape(sequences, 4, memory_width)
    input_pre = jnp.dot(normed, ingate_weight, preferred_element_type=jnp.float32) + ingate_bias
    forget_pre = jnp.dot(normed, forget_weight, preferred_element_type=jnp.float32) + forget_bias
    gated_out, next_memory, next_normalizer, next_stabilizer = memory_step(
        projected[:, 0],
        projected[:, 1],
        projected[:, 2],
        projected[:, 3],
        input_pre,
        forget_pre,
        memory_state,
        normalizer,
        stabilizer,
    )
    mixed_cols = mix(devices, gated_out, output_weight)
    mixed = jnp.swapaxes(mixed_cols, 0, 1).reshape(sequences, model_width)
    after_mix = rounded(residual + rms_scale(mixed.astype(jnp.float32), postmix_gain))
    after_float = after_mix.astype(jnp.float32)
    expert_input = rms_scale(after_float, prefeed_gain).astype(jnp.bfloat16)
    local_count = expert_gate.shape[0]
    experts_total = local_count * devices
    choose_count = expert_ids.shape[1]
    capacity = min(
        sequences, max(2, 2 * ((sequences * choose_count + experts_total - 1) // experts_total))
    )
    named = (expert_ids[:, :, None] == jnp.arange(experts_total, dtype=jnp.int32)).astype(
        jnp.float32
    )
    chosen = jnp.sum(named, axis=1)
    weight_of = jnp.sum(named * route_weights[:, :, None], axis=1)
    order = jnp.arange(sequences)
    before = (order[:, None] > order[None, :]).astype(jnp.float32)
    earlier = jnp.sum(before[:, :, None] * chosen[None, :, :], axis=1)
    slots = jnp.where(
        earlier[:, :, None] == jnp.arange(capacity, dtype=jnp.float32), chosen[:, :, None], 0.0
    )
    combine = (slots * weight_of[:, :, None]).reshape(sequences, experts_total * capacity)
    dispatch = slots.reshape(sequences, experts_total * capacity).T.astype(jnp.bfloat16)
    combined = experts(
        devices,
        expert_input,
        dispatch,
        combine,
        expert_gate,
        expert_up,
        expert_down,
        shared_gate,
        shared_up,
        shared_down,
    )
    next_tokens = (after_float + rms_scale(combined, postfeed_gain)).astype(jnp.bfloat16)
    return (next_tokens, next_memory, next_normalizer, next_stabilizer)


def solution(mesh):
    in_specs = (
        P("ep", None),
        P(),
        P(),
        P(),
        P(),
        P("ep", None),
        P("ep", None),
        P("ep", None),
        P("ep", None),
        P(),
        P(),
        P(),
        P(),
        P("ep", None, None, None),
        P("ep", None, None),
        P("ep", None),
        P(None, "ep"),
        P("ep", None),
        P("ep", None),
        P("ep", None, None),
        P("ep", None, None),
        P("ep", None, None),
        P(),
        P(),
        P(),
    )
    out_specs = (P("ep", None), P("ep", None, None, None), P("ep", None, None), P("ep", None))
    return jax.shard_map(
        on_device, mesh=mesh, in_specs=in_specs, out_specs=out_specs, check_vma=False
    )
```

time: 196 us -> 129 us (0.66)
  the two profiles are of different devices: /device:TPU:0 before, /device:TPU:29 now
where the time goes in v1:
time: 129 us
  Pallas kernels  102 us (79%)
  other arithmetic  11.8 us (9%)
  matrix products  10 us (8%)
  local copies, waits for them, and re-layouts  4.2 us (3%)
    pallas_call x1, Pallas kernels, project(): pl.pallas_call(functools.partial(project_kernel, n, groups), out_shape=ja...  46.1 us
    pallas_call x1, Pallas kernels, experts(): pl.pallas_call(functools.partial(expert_kernel, n), out_shape=jax.ShapeDt...  32.4 us
    pallas_call x1, Pallas kernels, mix(): pl.pallas_call(functools.partial(mix_kernel, n), out_shape=jax.ShapeDtype...  23.1 us
    dot_general x1, matrix products, memory_step(): jnp.einsum('shvk,shk->shv', memory_state, query_heads, precision=lax.Prec...  8.31 us
    add x1, other arithmetic, memory_step(): keep_old[..., None, None] * memory_state  2.8 us

profile of v1, /device:TPU:29, one launch (start us, length us, event | category | flops | bytes accessed | tf_op | source)
XLA Modules:
  0.0 128.6 jit_solution(10338451754046953827)
XLA Ops:
  0.6 0.0 copy-start
  0.6 0.0 copy-start.4
  0.7 0.0 copy-start.6
  0.7 0.0 copy-start.5
  0.7 0.0 copy-start.8
  0.7 0.9 fusion.2
  1.6 0.8 copy.70
  2.4 0.8 copy.75
  3.2 0.1 select_reduce_fusion
  3.3 0.1 multiply_reduce_fusion.1
  3.4 0.1 copy.73
  3.4 0.0 copy-start.9
  3.4 0.1 copy.71
  3.5 0.1 copy.76
  3.6 0.1 eq.40
  3.7 0.0 copy-start.1
  3.7 1.0 fusion.4.normed_ref
  4.7 0.0 copy-start.3
  4.7 0.9 fusion.23
  5.6 0.0 copy-done
  5.7 0.8 broadcast_multiply_fusion.2
  6.5 0.0 copy-start.7
  6.5 0.1 copy.79
  6.8 0.1 copy.78.dispatch_ref
  6.9 0.0 copy-done.3
  6.9 46.1 %shard_map.264 = f32[8,4096]{1,0:T(8,128)} custom-call(bf16[8,2048]{1,0:T(8,128)(2,1)} %copy-done.3, bf16[64,1024]{1,0:T(8,128)(2,1)} %query_ref.1, bf16[64,1024]{1,0:T(8,128)(2,1)} %key_ref.1, bf16[64,1024]{1,0:T(8,128)(2,1)} %value_ref.1, bf16[64,1024]{1,0:T(8,128)(2,1)} %gate_ref.1), custom_call_target="tpu_custom_call" | custom-call | tf_op jit(solution)/shard_map/pallas_call | solution.py:158
  53.1 0.9 broadcast_multiply_fusion
  54.0 0.1 copy.65
  54.1 0.8 slice_bitcast_fusion.1
  54.9 0.8 fusion.18
  55.7 8.3 %fusion.15 = f32[8,8,1,128]{3,2,1,0:T(1,128)S(1)} fusion(f32[8,8,128,128]{3,2,1,0:T(8,128)} %param.38, f32[8,8,128,1]{2,0,1,3:T(8,128)S(1)} %get-tuple-element.13), kind=kOutput, calls=%fused_computation.31 | convolution fusion | flops 12582912 | bytes 4259840 | tf_op jit(solution)/shard_map/shvk,shk->shv/dot_general | solution.py:356
  64.0 0.0 copy-done.6
  64.0 0.7 fusion.17
  64.8 1.4 %fusion.10.gated_ref = bf16[8,1024]{1,0:T(8,128)(2,1)} fusion(f32[1,8,8,128]{3,2,1,0:T(8,128)S(1)} %get-tuple-element.20, f32[8,4,1024]{2,0,1:T(8,128)} %bitcast.44), kind=kLoop, calls=%fused_computation.23 | loop fusion | flops 40960 | bytes 81920 | tf_op jit(solution)/shard_map/convert_element_type | solution.py:365
  66.2 0.0 copy-done.5
  66.2 0.8 copy.68.weight_ref
  67.0 23.1 %shard_map.265 = bf16[32,8,64]{2,1,0:T(8,128)(2,1)} custom-call(bf16[8,1024]{1,0:T(8,128)(2,1)} %fusion.10.gated_ref, bf16[1024,64]{1,0:T(8,128)(2,1)} %copy.68.weight_ref), custom_call_target="tpu_custom_call" | custom-call | tf_op jit(solution)/shard_map/pallas_call | solution.py:211
  90.1 1.0 fusion.1
  91.1 0.9 convert_bitcast_fusion
  92.0 0.1 reshape.111
  92.1 0.0 copy-done.4
  92.1 0.0 copy-done.8
  92.1 0.1 fusion.5
  92.2 0.1 fusion.6
  92.3 0.0 copy-done.9
  92.3 0.1 fusion.8.rows_ref
  92.4 0.0 copy-done.1
  92.4 0.0 copy-start.10
  92.4 0.0 copy-start.2
  92.5 32.4 %shard_map.266 = f32[8,2048]{1,0:T(8,128)S(1)} custom-call(bf16[8,2048]{1,0:T(8,128)(2,1)S(1)} %fusion.8.rows_ref, bf16[128,8]{1,0:T(8,128)(2,1)S(1)} %copy.78.dispatch_ref, f32[8,128]{1,0:T(8,128)S(1)} %fusion.25.combine_ref, bf16[1,2048,512]{2,1,0:T(8,128)(2,1)S(1)} %copy-done.1, bf16[1,2048,512]{2,1,0:T(8,128)(2,1)} %refs_1_.1, ...), custom_call_target="tpu_custom_call" | custom-call | tf_op jit(solution)/shard_map/pallas_call | solution.py:314
  124.9 0.0 copy-done.7
  124.9 0.1 multiply_reduce_fusion
  125.1 0.0 copy-done.10
  125.1 0.7 fusion.9
  125.8 0.0 copy-done.2
  125.8 2.8 %multiply_add_fusion = f32[8,8,128,128]{3,2,1,0:T(8,128)} fusion(f32[8,8,128,128]{3,2,1,0:T(8,128)S(1)} %copy-done.2, f32[8,8,128]{2,1,0:T(8,128)S(1)} %copy.81, f32[8,8,128]{2,1,0:T(8,128)S(1)} %copy.80, f32[8,8]{1,0:T(8,128)S(1)} %get-tuple-element.10), kind=kLoop, calls=%fused_computation | loop fusion | flops 3145728 | bytes 8454400 | tf_op jit(solution)/shard_map/add | solution.py:367
  (18 shorter events, 0.3 us)
Async XLA Ops:
  0.6 5.0 %copy-start = (bf16[2048,8]{0,1:T(8,128)(2,1)S(1)}, bf16[2048,8]{0,1:T(8,128)(2,1)}, u32[]{:S(2)}) copy-start(bf16[2048,8]{0,1:T(8,128)(2,1)} %param.34) | copy-start | bytes 98308
  0.6 91.5 %copy-start.4 = (bf16[8,2048]{1,0:T(8,128)(2,1)S(1)}, bf16[8,2048]{1,0:T(8,128)(2,1)}, u32[]{:S(2)}) copy-start(bf16[8,2048]{1,0:T(8,128)(2,1)} %param.25) | copy-start | bytes 98308
  0.7 63.4 %copy-start.6 = (f32[8,8,128]{2,1,0:T(8,128)S(1)}, f32[8,8,128]{2,1,0:T(8,128)}, u32[]{:S(2)}) copy-start(f32[8,8,128]{2,1,0:T(8,128)} %param.39) | copy-start | bytes 98308
  0.7 65.5 %copy-start.5 = (bf16[1024,64]{0,1:T(8,128)(2,1)S(1)}, bf16[1024,64]{0,1:T(8,128)(2,1)}, u32[]{:S(2)}) copy-start(bf16[1024,64]{0,1:T(8,128)(2,1)} %param.41) | copy-start | bytes 393220
  0.7 91.4 %copy-start.8 = (f32[2048]{0:T(1024)S(1)}, f32[2048]{0:T(1024)}, u32[]{:S(2)}) copy-start(f32[2048]{0:T(1024)} %param.27) | copy-start | bytes 24580
  3.4 88.9 %copy-start.9 = (f32[2048]{0:T(1024)S(1)}, f32[2048]{0:T(1024)}, u32[]{:S(2)}) copy-start(f32[2048]{0:T(1024)} %param.28) | copy-start | bytes 24580
  3.7 88.7 %copy-start.1 = (bf16[1,2048,512]{2,1,0:T(8,128)(2,1)S(1)}, bf16[1,2048,512]{2,1,0:T(8,128)(2,1)}, u32[]{:S(2)}) copy-start(bf16[1,2048,512]{2,1,0:T(8,128)(2,1)} %refs_0_.1) | copy-start | bytes 6291460
  4.7 2.2 %copy-start.3 = (bf16[8,2048]{1,0:T(8,128)(2,1)}, bf16[8,2048]{1,0:T(8,128)(2,1)S(1)}, u32[]{:S(2)}) copy-start(bf16[8,2048]{1,0:T(8,128)(2,1)S(1)} %fusion.4.normed_ref) | copy-start | bytes 98308
  6.5 118.5 %copy-start.7 = (f32[8,8]{1,0:T(8,128)}, f32[8,8]{1,0:T(8,128)S(1)}, u32[]{:S(2)}) copy-start(f32[8,8]{1,0:T(8,128)S(1)} %get-tuple-element.8) | copy-start | bytes 772
  92.4 32.6 %copy-start.10 = (f32[2048]{0:T(1024)S(1)}, f32[2048]{0:T(1024)}, u32[]{:S(2)}) copy-start(f32[2048]{0:T(1024)} %param.29) | copy-start | bytes 24580
  92.4 33.3 %copy-start.2 = (f32[8,8,128,128]{3,2,1,0:T(8,128)S(1)}, f32[8,8,128,128]{3,2,1,0:T(8,128)}, u32[]{:S(2)}) copy-start(f32[8,8,128,128]{3,2,1,0:T(8,128)} %param.38) | copy-start | bytes 12582916

commit v2 on v1

--- a/solution.py
+++ b/solution.py
@@ -9,6 +9,7 @@
 
 epsilon = 1e-06
 LANES = 128
+GROUPS = 4
 MESH = pl.DeviceIdType.MESH
 VM = pl.BlockSpec(memory_space=pltpu.VMEM)
 ANY = pl.BlockSpec(memory_space=pl.ANY)
@@ -63,7 +64,9 @@
     key_ref,
     value_ref,
     gate_ref,
+    mix_ref,
     out_ref,
+    mix_all_ref,
     rows_buf,
     weight_buf,
     product_buf,
@@ -72,156 +75,118 @@
     recv_sems,
 ):
     me = lax.axis_index("ep")
-    blocks = n // groups
-    per_matrix = blocks // 4
-    mine, turn = me // groups, lax.rem(me, groups)
+    members = n // groups
+    plane, place = me // members, lax.rem(me, members)
+    width = rows_buf.shape[2]
+    columns = weight_buf.shape[2]
+    per_matrix = query_ref.shape[1] // columns
     greet(n, me)
     weights = (query_ref, key_ref, value_ref, gate_ref)
 
     def column(block):
-        return pl.ds(pl.multiple_of(lax.rem(block, per_matrix) * LANES, LANES), LANES)
+        return pl.ds(pl.multiple_of(lax.rem(block, per_matrix) * columns, LANES), columns)
+
+    def part(index):
+        return normed_ref.at[:, pl.ds(pl.multiple_of(index * width, LANES), width)]
 
     for index, ref in enumerate(weights):
 
-        @pl.when(mine // per_matrix == index)
+        @pl.when(place // per_matrix == index)
         def _():
             pltpu.make_async_copy(
-                ref.at[:, column(mine)], weight_buf.at[me], recv_sems.at[1]
+                ref.at[:, column(place)], weight_buf.at[place], recv_sems.at[1]
             ).start()
 
-    pltpu.make_async_copy(normed_ref, rows_buf.at[mine], recv_sems.at[0]).start()
+    pltpu.make_async_copy(part(plane), rows_buf.at[me], recv_sems.at[0]).start()
+    pltpu.make_async_copy(mix_ref, mix_all_ref.at[place], recv_sems.at[3]).start()
     greeted(n)
 
     def send_rows(i, carry):
-        place = lax.rem(mine + i, blocks)
+        peer = lax.rem(me + i, n)
         send(
-            normed_ref,
-            rows_buf.at[mine],
-            send_sems.at[0],
-            recv_sems.at[0],
-            place * groups + turn,
+            part(peer // members), rows_buf.at[me], send_sems.at[0], recv_sems.at[0], peer
         )
         return carry
 
     def send_weights(i, carry):
-        peer = lax.rem(me + i, n)
-        block = peer // groups
+        block = lax.rem(place + i, members)
         for index, ref in enumerate(weights):
 
             @pl.when(block // per_matrix == index)
             def _():
                 send(
                     ref.at[:, column(block)],
-                    weight_buf.at[me],
+                    weight_buf.at[place],
                     send_sems.at[1],
                     recv_sems.at[1],
-                    peer,
+                    plane * members + block,
                 )
 
         return carry
 
-    lax.fori_loop(1, n, send_weights, 0)
-    lax.fori_loop(1, blocks, send_rows, 0)
+    lax.fori_loop(1, members, send_weights, 0)
+    lax.fori_loop(1, n, send_rows, 0)
     drain(rows_buf, recv_sems.at[0])
     drain(weight_buf, recv_sems.at[1])
-    rows = rows_buf[...].reshape(rows_buf.shape[0] * rows_buf.shape[1], rows_buf.shape[2])
-    weight = weight_buf[...].reshape(weight_buf.shape[0] * weight_buf.shape[1], LANES)
+    rows = rows_buf[...].reshape(rows_buf.shape[0] * rows_buf.shape[1], width)
+    weight = weight_buf[...].reshape(weight_buf.shape[0] * weight_buf.shape[1], columns)
     product = jnp.dot(rows, weight, preferred_element_type=jnp.float32)
     product_buf[...] = product.reshape(product_buf.shape).astype(jnp.bfloat16)
-    pltpu.make_async_copy(product_buf.at[mine], result_buf.at[mine], recv_sems.at[2]).start()
+    pltpu.make_async_copy(product_buf.at[me], result_buf.at[me], recv_sems.at[2]).start()
 
     def send_product(i, carry):
-        place = lax.rem(mine + i, blocks)
+        peer = lax.rem(me + i, n)
+        send(product_buf.at[peer], result_buf.at[me], send_sems.at[2], recv_sems.at[2], peer)
+        return carry
+
+    def send_mix(i, carry):
         send(
-            product_buf.at[place],
-            result_buf.at[mine],
-            send_sems.at[2],
-            recv_sems.at[2],
-            place * groups + turn,
+            mix_ref,
+            mix_all_ref.at[place],
+            send_sems.at[3],
+            recv_sems.at[3],
+            plane * members + lax.rem(place + i, members),
         )
         return carry
 
-    lax.fori_loop(1, blocks, send_product, 0)
+    lax.fori_loop(1, n, send_product, 0)
+    lax.fori_loop(1, members, send_mix, 0)
     drain(result_buf, recv_sems.at[2])
-    for block in range(blocks):
-        out_ref[:, block * LANES : (block + 1) * LANES] = result_buf[block].astype(jnp.float32)
-    drain(rows_buf.at[pl.ds(0, blocks - 1)], send_sems.at[0])
-    drain(weight_buf.at[pl.ds(0, n - 1)], send_sems.at[1])
-    drain(result_buf.at[pl.ds(0, blocks - 1)], send_sems.at[2])
-
-
-def project(n, normed, *weights):
+    for member in range(members):
+        total = result_buf[member].astype(jnp.float32)
+        for group in range(1, groups):
+            total = total + result_buf[group * members + member].astype(jnp.float32)
+        out_ref[:, member * columns : (member + 1) * columns] = total
+    drain(mix_all_ref, recv_sems.at[3])
+    drain(rows_buf.at[pl.ds(0, n - 1)], send_sems.at[0])
+    drain(weight_buf.at[pl.ds(0, members - 1)], send_sems.at[1])
+    drain(result_buf.at[pl.ds(0, n - 1)], send_sems.at[2])
+    drain(mix_all_ref.at[pl.ds(0, members - 1)], send_sems.at[3])
+
+
+def project(n, groups, normed, mix_weight, *weights):
     sequences, width = normed.shape
     depth, columns = weights[0].shape
-    blocks = 4 * columns // LANES
-    groups = n // blocks
+    members = n // groups
+    wide = 4 * columns // members
     return pl.pallas_call(
         functools.partial(project_kernel, n, groups),
-        out_shape=jax.ShapeDtypeStruct((sequences, 4 * columns), jnp.float32),
-        in_specs=[VM, ANY, ANY, ANY, ANY],
-        out_specs=VM,
+        out_shape=(
+            jax.ShapeDtypeStruct((sequences, 4 * columns), jnp.float32),
+            jax.ShapeDtypeStruct((members,) + mix_weight.shape, jnp.bfloat16),
+        ),
+        in_specs=[VM, ANY, ANY, ANY, ANY, VM],
+        out_specs=(VM, ANY),
         scratch_shapes=[
-            pltpu.VMEM((blocks, sequences, width), jnp.bfloat16),
-            pltpu.VMEM((n, depth, LANES), jnp.bfloat16),
-            pltpu.VMEM((blocks, sequences, LANES), jnp.bfloat16),
-            pltpu.VMEM((blocks, sequences, LANES), jnp.bfloat16),
-            pltpu.SemaphoreType.DMA((3,)),
-            pltpu.SemaphoreType.DMA((3,)),
+            pltpu.VMEM((n, sequences, width // groups), jnp.bfloat16),
+            pltpu.VMEM((members, depth, wide), jnp.bfloat16),
+            pltpu.VMEM((n, sequences, wide), jnp.bfloat16),
+            pltpu.VMEM((n, sequences, wide), jnp.bfloat16),
+            pltpu.SemaphoreType.DMA((4,)),
+            pltpu.SemaphoreType.DMA((4,)),
         ],
         compiler_params=pltpu.CompilerParams(collective_id=0, has_side_effects=True),
-    )(normed, *weights)
-
-
-def mix_kernel(
-    n, gated_ref, weight_ref, out_ref, rows_buf, product_buf, result_buf, send_sems, recv_sems
-):
-    me = lax.axis_index("ep")
-    greet(n, me)
-    pltpu.make_async_copy(gated_ref, rows_buf.at[me], recv_sems.at[0]).start()
-    greeted(n)
-
-    def send_rows(i, carry):
-        send(
-            gated_ref, rows_buf.at[me], send_sems.at[0], recv_sems.at[0], lax.rem(me + i, n)
-        )
-        return carry
-
-    lax.fori_loop(1, n, send_rows, 0)
-    drain(rows_buf, recv_sems.at[0])
-    rows = rows_buf[...].reshape(rows_buf.shape[0] * rows_buf.shape[1], rows_buf.shape[2])
-    product = jnp.dot(rows, weight_ref[...], preferred_element_type=jnp.float32)
-    product_buf[...] = product.reshape(product_buf.shape).astype(jnp.bfloat16)
-    pltpu.make_async_copy(product_buf.at[me], result_buf.at[me], recv_sems.at[1]).start()
-
-    def send_product(i, carry):
-        peer = lax.rem(me + i, n)
-        send(product_buf.at[peer], result_buf.at[me], send_sems.at[1], recv_sems.at[1], peer)
-        return carry
-
-    lax.fori_loop(1, n, send_product, 0)
-    drain(result_buf, recv_sems.at[1])
-    out_ref[...] = result_buf[...]
-    drain(rows_buf.at[pl.ds(0, n - 1)], send_sems.at[0])
-    drain(result_buf.at[pl.ds(0, n - 1)], send_sems.at[1])
-
-
-def mix(n, gated, weight):
-    sequences, width = gated.shape
-    columns = weight.shape[1]
-    return pl.pallas_call(
-        functools.partial(mix_kernel, n),
-        out_shape=jax.ShapeDtypeStruct((n, sequences, columns), jnp.bfloat16),
-        in_specs=[VM, VM],
-        out_specs=VM,
-        scratch_shapes=[
-            pltpu.VMEM((n, sequences, width), jnp.bfloat16),
-            pltpu.VMEM((n, sequences, columns), jnp.bfloat16),
-            pltpu.VMEM((n, sequences, columns), jnp.bfloat16),
-            pltpu.SemaphoreType.DMA((2,)),
-            pltpu.SemaphoreType.DMA((2,)),
-        ],
-        compiler_params=pltpu.CompilerParams(collective_id=1, has_side_effects=True),
-    )(gated, weight)
+    )(normed, *weights, mix_weight)
 
 
 def two_layer(rows, gate_weight, up_weight, down_weight):
@@ -231,33 +196,87 @@
     return jnp.dot(inner_rows, down_weight, preferred_element_type=jnp.float32)
 
 
-def expert_kernel(
+def tail_kernel(
     n,
-    rows_ref,
+    groups,
+    gated_ref,
+    tokens_ref,
+    postmix_ref,
+    prefeed_ref,
+    postfeed_ref,
     dispatch_ref,
     combine_ref,
     *refs,
 ):
-    weights_hbm, out_ref = refs[:6], refs[6]
-    weights, (outgoing, arrived, answer, returned, load_sems, send_sems, recv_sems) = (
-        refs[7:13],
-        refs[13:],
+    weights_hbm, out_ref = refs[:7], refs[7]
+    weights, (
+        gated_buf,
+        product_buf,
+        mixed_buf,
+        outgoing,
+        arrived,
+        answer,
+        returned,
+        load_sems,
+        send_sems,
+        recv_sems,
+    ) = (
+        refs[8:15],
+        refs[15:],
     )
     me = lax.axis_index("ep")
+    members = n // groups
+    plane, place = me // members, lax.rem(me, members)
     greet(n, me)
     loads = [
         pltpu.make_async_copy(source, target, load_sems.at[index])
         for index, (source, target) in enumerate(zip(weights_hbm, weights))
     ]
-    for index in (3, 4, 5, 0, 1, 2):
+    for index in (6, 3, 4, 5, 0, 1, 2):
         loads[index].start()
+    pltpu.make_async_copy(gated_ref, gated_buf.at[plane], recv_sems.at[2]).start()
+    greeted(n)
+
+    def line(source, target, stage):
+        for i in range(1, groups):
+            peer = lax.rem(plane + i, groups)
+            send(
+                source(peer),
+                target.at[plane],
+                send_sems.at[stage],
+                recv_sems.at[stage],
+                peer * members + place,
+            )
+
+    line(lambda peer: gated_ref, gated_buf, 2)
+    loads[6].wait()
+    drain(gated_buf, recv_sems.at[2])
+    gated = gated_buf[...].reshape(gated_buf.shape[0] * gated_buf.shape[1], gated_buf.shape[2])
+    mix_weight = weights[6][...]
+    mix_weight = mix_weight.reshape(mix_weight.shape[0] * mix_weight.shape[1], mix_weight.shape[2])
+    product_buf[...] = (
+        lax.dot_general(
+            gated, mix_weight, (((1,), (1,)), ((), ())), preferred_element_type=jnp.float32
+        )
+        .reshape(product_buf.shape)
+        .astype(jnp.bfloat16)
+    )
+    pltpu.make_async_copy(product_buf.at[plane], mixed_buf.at[plane], recv_sems.at[3]).start()
+    line(lambda peer: product_buf.at[peer], mixed_buf, 3)
+    drain(mixed_buf, recv_sems.at[3])
+    mixed = jnp.concatenate([mixed_buf[group] for group in range(groups)], axis=1)
+    after_mix = (
+        tokens_ref[...].astype(jnp.float32)
+        + rms_scale(mixed.astype(jnp.float32), postmix_ref[...])
+    ).astype(jnp.bfloat16)
+    after_float = after_mix.astype(jnp.float32)
+    token_rows = rms_scale(after_float, prefeed_ref[...]).astype(jnp.bfloat16)
     local, capacity = weights[0].shape[0], outgoing.shape[2]
-    width = rows_ref.shape[1]
+    width = token_rows.shape[1]
     outgoing[...] = jnp.dot(
-        dispatch_ref[...], rows_ref[...], preferred_element_type=jnp.float32
+        dispatch_ref[...], token_rows, preferred_element_type=jnp.float32
     ).reshape(outgoing.shape).astype(jnp.bfloat16)
     pltpu.make_async_copy(outgoing.at[me], arrived.at[me], recv_sems.at[0]).start()
-    greeted(n)
 
     def exchange(source, target, stage):
         def one(i, carry):
@@ -271,7 +290,7 @@
     for index in (3, 4, 5):
         loads[index].wait()
     shared_out = two_layer(
-        rows_ref[...], weights[3][...], weights[4][...], weights[5][...]
+        token_rows, weights[3][...], weights[4][...], weights[5][...]
     )
     for index in (0, 1, 2):
         loads[index].wait()
@@ -297,36 +316,41 @@
     picked = (
         returned[...].astype(jnp.float32).reshape(combine.shape[1], width).astype(jnp.bfloat16)
     )
-    out_ref[...] = (
+    combined = (
         shared_out
         + jnp.dot(high, picked, preferred_element_type=jnp.float32)
         + jnp.dot(low, picked, preferred_element_type=jnp.float32)
     )
+    out_ref[...] = (after_float + rms_scale(combined, postfeed_ref[...])).astype(jnp.bfloat16)
     drain(arrived.at[pl.ds(0, n - 1)], send_sems.at[0])
     drain(returned.at[pl.ds(0, n - 1)], send_sems.at[1])
-
-
-def experts(n, rows, dispatch, combine, *weights):
-    sequences, width = rows.shape
+    drain(gated_buf.at[pl.ds(0, groups - 1)], send_sems.at[2])
+    drain(mixed_buf.at[pl.ds(0, groups - 1)], send_sems.at[3])
+
+
+def tail(n, groups, gated, tokens, gains, dispatch, combine, *weights):
+    sequences, width = tokens.shape
     local = weights[0].shape[0]
     capacity = dispatch.shape[0] // (n * local)
     slots = pltpu.VMEM((n, local, capacity, width), jnp.bfloat16)
+    pieces = pltpu.VMEM((groups, sequences, width // groups), jnp.bfloat16)
     return pl.pallas_call(
-        functools.partial(expert_kernel, n),
-        out_shape=jax.ShapeDtypeStruct((sequences, width), jnp.float32),
-        in_specs=[VM, VM, VM] + [ANY] * 6,
+        functools.partial(tail_kernel, n, groups),
+        out_shape=jax.ShapeDtypeStruct((sequences, width), jnp.bfloat16),
+        in_specs=[VM] * 7 + [ANY] * 7,
         out_specs=VM,
         scratch_shapes=[pltpu.VMEM(w.shape, w.dtype) for w in weights]
+        + [pltpu.VMEM((groups,) + gated.shape, jnp.bfloat16), pieces, pieces]
         + [slots] * 4
         + [
-            pltpu.SemaphoreType.DMA((6,)),
-            pltpu.SemaphoreType.DMA((2,)),
-            pltpu.SemaphoreType.DMA((2,)),
+            pltpu.SemaphoreType.DMA((7,)),
+            pltpu.SemaphoreType.DMA((4,)),
+            pltpu.SemaphoreType.DMA((4,)),
         ],
         compiler_params=pltpu.CompilerParams(
             collective_id=2, has_side_effects=True, vmem_limit_bytes=50 * 1024 * 1024
         ),
-    )(rows, dispatch, combine, *weights)
+    )(gated, tokens, *(gain[None] for gain in gains), dispatch, combine, *weights)
 
 
 def memory_step(
@@ -404,7 +428,9 @@
     devices = lax.axis_size("ep")
     residual = tokens.astype(jnp.float32)
     normed = rms_scale(residual, premix_gain).astype(jnp.bfloat16)
-    projected = project(devices, normed, query_weight, key_weight, value_weight, outgate_weight)
+    projected, mix_weight = project(
+        devices, GROUPS, normed, output_weight.T, query_weight, key_weight, value_weight, outgate_weight
+    )
     projected = projected.reshape(sequences, 4, memory_width)
     input_pre = jnp.dot(normed, ingate_weight, preferred_element_type=jnp.float32) + ingate_bias
     forget_pre = jnp.dot(normed, forget_weight, preferred_element_type=jnp.float32) + forget_bias
@@ -419,11 +445,6 @@
         normalizer,
         stabilizer,
     )
-    mixed_cols = mix(devices, gated_out, output_weight)
-    mixed = jnp.swapaxes(mixed_cols, 0, 1).reshape(sequences, model_width)
-    after_mix = rounded(residual + rms_scale(mixed.astype(jnp.float32), postmix_gain))
-    after_float = after_mix.astype(jnp.float32)
-    expert_input = rms_scale(after_float, prefeed_gain).astype(jnp.bfloat16)
     local_count = expert_gate.shape[0]
     experts_total = local_count * devices
     choose_count = expert_ids.shape[1]
@@ -443,9 +464,12 @@
     )
     combine = (slots * weight_of[:, :, None]).reshape(sequences, experts_total * capacity)
     dispatch = slots.reshape(sequences, experts_total * capacity).T.astype(jnp.bfloat16)
-    combined = experts(
+    next_tokens = tail(
         devices,
-        expert_input,
+        GROUPS,
+        gated_out,
+        tokens,
+        (postmix_gain, prefeed_gain, postfeed_gain),
         dispatch,
         combine,
         expert_gate,
@@ -454,8 +478,8 @@
         shared_gate,
         shared_up,
         shared_down,
-    )
-    next_tokens = (after_float + rms_scale(combined, postfeed_gain)).astype(jnp.bfloat16)
+        mix_weight,
+    )
     return (next_tokens, next_memory, next_normalizer, next_stabilizer)
 
 

time: 129 us -> 94.4 us (0.73)
  Pallas kernels: 102 us -> 70.8 us
  other arithmetic: 11.8 us -> 8.23 us
    pallas_call x3 -> x2, Pallas kernels: 102 us -> 70.8 us  [the longest x1 39.3 us: tail(): pl.pallas_call(functools.partial(tail_kernel, n, groups), out_shape=jax.S...]
    convert_element_type x4 -> x0, other arithmetic: 1.71 us -> none  [the longest x1 0.86 us: on_device(): mixed.astype(jnp.float32)]
where the time goes in v2:
time: 94.4 us; the launch traced here: 93.8 us
  Pallas kernels  70.8 us (75%)
  matrix products  10 us (11%)
  other arithmetic  8.23 us (9%)
  local copies, waits for them, and re-layouts  3.85 us (4%)
    pallas_call x1, Pallas kernels, tail(): pl.pallas_call(functools.partial(tail_kernel, n, groups), out_shape=jax.S...  39.3 us
    pallas_call x1, Pallas kernels, project(): pl.pallas_call(functools.partial(project_kernel, n, groups), out_shape=(j...  31.5 us
    dot_general x1, matrix products, memory_step(): jnp.einsum('shvk,shk->shv', memory_state, query_heads, precision=lax.Prec...  8.31 us
    add x1, other arithmetic, memory_step(): keep_old[..., None, None] * memory_state  2.82 us
    unnamed x25, local copies, waits for them, and re-layouts  2.21 us

profile of v2, /device:TPU:29, one launch (start us, length us, event | category | flops | bytes accessed | tf_op | source)
XLA Modules:
  0.0 93.8 jit_solution(10275922502636907459)
XLA Ops:
  0.6 0.0 copy-start
  0.6 0.0 copy-start.3
  0.7 0.0 copy-start.9
  0.7 0.0 copy-start.1
  0.7 0.0 copy-start.6
  0.7 0.0 copy-start.5
  0.7 0.0 copy-start.4
  0.7 1.0 %fusion.1 = f32[8]{0:T(128)S(1)} fusion(bf16[8,2048]{1,0:T(8,128)(2,1)} %tokens_ref.1), kind=kLoop, calls=%fused_computation.6 | loop fusion | flops 49144 | bytes 32800 | tf_op jit(solution)/shard_map/reduce_sum | solution.py:20
  1.8 0.8 copy.62
  2.5 0.8 copy.67
  3.3 0.1 select_reduce_fusion
  3.4 0.1 multiply_reduce_fusion
  3.5 0.1 copy.65
  3.6 0.1 copy.63
  3.6 0.1 copy.68
  3.7 0.1 eq.40
  3.8 0.8 fusion.3.normed_ref
  4.7 0.0 copy-start.8
  4.7 0.9 fusion.17
  5.6 0.0 copy-done
  5.6 0.8 broadcast_multiply_fusion.2
  6.4 0.0 copy-start.10
  6.4 0.1 copy.71
  6.8 0.1 copy.70.dispatch_ref
  6.9 0.0 copy-done.8
  6.9 31.5 %shard_map.264 = (f32[8,4096]{1,0:T(8,128)}, bf16[8,64,1024]{2,1,0:T(8,128)(2,1)}) custom-call(bf16[8,2048]{1,0:T(8,128)(2,1)} %copy-done.8, bf16[64,1024]{1,0:T(8,128)(2,1)} %query_ref.1, bf16[64,1024]{1,0:T(8,128)(2,1)} %key_ref.1, bf16[64,1024]{1,0:T(8,128)(2,1)} %value_ref.1, bf16[64,1024]{1,0:T(8,128)(2,1)} %gate_ref.1, bf16[64,1024]{1,0:T(8,128)(2,1)} %bitcast.54), custom_call_target="tpu_custom_call" | custom-call | tf_op jit(solution)/shard_map/pallas_call | solution.py:172
  38.4 0.0 copy-start.2
  38.4 1.0 %broadcast_multiply_fusion = (f32[8,8,128]{2,0,1:T(8,128)S(1)}, f32[8,8,128]{2,0,1:T(8,128)S(1)}, f32[8,8]{0,1:T(8,128)S(1)}) fusion(f32[8,8]{0,1:T(8,128)S(1)} %copy.71, f32[8,4,1024]{2,0,1:T(8,128)} %bitcast.47), kind=kLoop, calls=%fused_computation.35 | loop fusion | flops 32704 | bytes 164352 | tf_op jit(solution)/shard_map/mul | solution.py:392
  39.4 0.1 copy.59
  39.5 0.8 slice_bitcast_fusion.1
  40.3 0.8 fusion.12
  41.1 8.3 %fusion.9 = f32[8,8,1,128]{3,2,1,0:T(1,128)S(1)} fusion(f32[8,8,128,128]{3,2,1,0:T(8,128)} %param.38, f32[8,8,128,1]{2,0,1,3:T(8,128)S(1)} %get-tuple-element.17), kind=kOutput, calls=%fused_computation.18 | convolution fusion | flops 12582912 | bytes 4259840 | tf_op jit(solution)/shard_map/shvk,shk->shv/dot_general | solution.py:380
  49.4 0.0 copy-done.9
  49.4 0.7 fusion.11
  50.2 0.8 fusion.4.gated_ref
  50.9 0.0 copy-done.3
  51.0 0.0 copy-done.1
  51.0 0.0 copy-done.6
  51.0 0.0 copy-done.5
  51.0 0.0 copy-done.4
  51.0 0.0 copy-done.2
  51.0 0.0 copy-start.7
  51.0 39.3 %shard_map.265 = bf16[8,2048]{1,0:T(8,128)(2,1)S(1)} custom-call(bf16[8,1024]{1,0:T(8,128)(2,1)S(1)} %fusion.4.gated_ref, bf16[8,2048]{1,0:T(8,128)(2,1)S(1)} %copy-done.3, f32[1,2048]{1,0:T(1,128)S(1)} %bitcast.44, f32[1,2048]{1,0:T(1,128)S(1)} %bitcast.45, f32[1,2048]{1,0:T(1,128)S(1)} %bitcast.46, bf16[128,8]{1,0:T(8,128)(2,1)S(1)} %copy.70.dispatch_ref, ...), custom_call_target="tpu_custom_call" | custom-call | tf_op jit(solution)/shard_map/pallas_call | solution.py:337
  90.4 0.0 copy-done.10
  90.4 0.0 copy-done.7
  90.4 2.8 %multiply_add_fusion = f32[8,8,128,128]{3,2,1,0:T(8,128)} fusion(f32[8,8,128,128]{3,2,1,0:T(8,128)S(1)} %copy-done.7, f32[8,8,128]{2,1,0:T(8,128)S(1)} %copy.73, f32[8,8,128]{2,1,0:T(8,128)S(1)} %copy.72, f32[8,8]{1,0:T(8,128)S(1)} %get-tuple-element.14), kind=kLoop, calls=%fused_computation | loop fusion | flops 3145728 | bytes 8454400 | tf_op jit(solution)/shard_map/add | solution.py:391
  93.2 0.6 copy.95
  (14 shorter events, 0.3 us)
Async XLA Ops:
  0.6 5.0 %copy-start = (bf16[2048,8]{0,1:T(8,128)(2,1)S(1)}, bf16[2048,8]{0,1:T(8,128)(2,1)}, u32[]{:S(2)}) copy-start(bf16[2048,8]{0,1:T(8,128)(2,1)} %param.34) | copy-start | bytes 98308
  0.6 50.3 %copy-start.3 = (bf16[8,2048]{1,0:T(8,128)(2,1)S(1)}, bf16[8,2048]{1,0:T(8,128)(2,1)}, u32[]{:S(2)}) copy-start(bf16[8,2048]{1,0:T(8,128)(2,1)} %tokens_ref.1) | copy-start | bytes 98308
  0.7 48.8 %copy-start.9 = (f32[8,8,128]{2,1,0:T(8,128)S(1)}, f32[8,8,128]{2,1,0:T(8,128)}, u32[]{:S(2)}) copy-start(f32[8,8,128]{2,1,0:T(8,128)} %param.39) | copy-start | bytes 98308
  0.7 50.3 %copy-start.1 = (bf16[1,2048,512]{2,1,0:T(8,128)(2,1)S(1)}, bf16[1,2048,512]{2,1,0:T(8,128)(2,1)}, u32[]{:S(2)}) copy-start(bf16[1,2048,512]{2,1,0:T(8,128)(2,1)} %refs_0_.1) | copy-start | bytes 6291460
  0.7 50.3 %copy-start.6 = (f32[2048]{0:T(1024)S(1)}, f32[2048]{0:T(1024)}, u32[]{:S(2)}) copy-start(f32[2048]{0:T(1024)} %param.29) | copy-start | bytes 24580
  0.7 50.3 %copy-start.5 = (f32[2048]{0:T(1024)S(1)}, f32[2048]{0:T(1024)}, u32[]{:S(2)}) copy-start(f32[2048]{0:T(1024)} %param.28) | copy-start | bytes 24580
  0.7 50.3 %copy-start.4 = (f32[2048]{0:T(1024)S(1)}, f32[2048]{0:T(1024)}, u32[]{:S(2)}) copy-start(f32[2048]{0:T(1024)} %param.27) | copy-start | bytes 24580
  4.7 2.2 %copy-start.8 = (bf16[8,2048]{1,0:T(8,128)(2,1)}, bf16[8,2048]{1,0:T(8,128)(2,1)S(1)}, u32[]{:S(2)}) copy-start(bf16[8,2048]{1,0:T(8,128)(2,1)S(1)} %fusion.3.normed_ref) | copy-start | bytes 98308
  6.4 83.9 %copy-start.10 = (f32[8,8]{1,0:T(8,128)}, f32[8,8]{1,0:T(8,128)S(1)}, u32[]{:S(2)}) copy-start(f32[8,8]{1,0:T(8,128)S(1)} %get-tuple-element.32) | copy-start | bytes 772
  38.4 12.6 %copy-start.2 = (bf16[8,64,1024]{2,1,0:T(8,128)(2,1)S(1)}, bf16[8,64,1024]{2,1,0:T(8,128)(2,1)}, u32[]{:S(2)}) copy-start(bf16[8,64,1024]{2,1,0:T(8,128)(2,1)} %get-tuple-element.7.refs_6_) | copy-start | bytes 3145732
  51.0 39.4 %copy-start.7 = (f32[8,8,128,128]{3,2,1,0:T(8,128)S(1)}, f32[8,8,128,128]{3,2,1,0:T(8,128)}, u32[]{:S(2)}) copy-start(f32[8,8,128,128]{3,2,1,0:T(8,128)} %param.38) | copy-start | bytes 12582916

commit v3 on v0

v3 whole, which is shorter than its diff:
```python
import functools

import jax
import jax.numpy as jnp
from jax import lax
from jax.experimental import pallas as pl
from jax.experimental.pallas import tpu as pltpu
from jax.sharding import PartitionSpec as P

epsilon = 1e-06
LANES = 128
GROUPS = 4
MESH = pl.DeviceIdType.MESH
VM = pl.BlockSpec(memory_space=pltpu.VMEM)
ANY = pl.BlockSpec(memory_space=pl.ANY)


def rms_scale(values, gain_row):
    return (
        values * lax.rsqrt(jnp.mean(values * values, axis=-1, keepdims=True) + epsilon) * gain_row
    )


def greet(n, me):
    sem = pltpu.get_barrier_semaphore()

    def signal(i, carry):
        pl.semaphore_signal(
            sem, inc=1, device_id=(lax.rem(me + i, n),), device_id_type=MESH
        )
        return carry

    lax.fori_loop(1, n, signal, 0)


def greeted(n):
    pl.semaphore_wait(pltpu.get_barrier_semaphore(), n - 1)


def send(src, dst, send_sem, recv_sem, peer):
    pltpu.make_async_remote_copy(
        src_ref=src,
        dst_ref=dst,
        send_sem=send_sem,
        recv_sem=recv_sem,
        device_id=(peer,),
        device_id_type=MESH,
    ).start()


def drain(ref, sem):
    pltpu.make_async_copy(ref, ref, sem).wait()


def routing(ids, route_weights, slot_count, capacity):
    sequences, choices = ids.shape
    slot = lax.broadcasted_iota(jnp.int32, (sequences, slot_count), 1).astype(jnp.float32)
    owner = jnp.floor((slot + 0.5) * (1.0 / capacity))
    turn = slot - owner * capacity
    chosen = jnp.zeros((sequences, slot_count), jnp.float32)
    weight_of = jnp.zeros((sequences, slot_count), jnp.float32)
    float_ids = ids.astype(jnp.float32)
    for choice in range(choices):
        same = float_ids[:, choice : choice + 1] == owner
        chosen = jnp.where(same, 1.0, chosen)
        weight_of = jnp.where(same, route_weights[:, choice : choice + 1], weight_of)
    earlier = jnp.zeros((sequences, slot_count), jnp.float32)
    row = lax.broadcasted_iota(jnp.int32, (sequences, slot_count), 0)
    for other in range(sequences - 1):
        earlier = earlier + jnp.where(row > other, chosen[other : other + 1], 0.0)
    slots = jnp.where(earlier == turn, chosen, 0.0)
    return slots, slots * weight_of


def two_layer(rows, gate_weight, up_weight, down_weight):
    gate_values = jnp.dot(rows, gate_weight, preferred_element_type=jnp.float32)
    up_values = jnp.dot(rows, up_weight, preferred_element_type=jnp.float32)
    inner_rows = (gate_values * jax.nn.sigmoid(gate_values) * up_values).astype(jnp.bfloat16)
    return jnp.dot(inner_rows, down_weight, preferred_element_type=jnp.float32)


def layer_kernel(n, groups, *refs):
    (
        tokens_ref,
        premix_ref,
        postmix_ref,
        prefeed_ref,
        postfeed_ref,
        input_bias_ref,
        forget_bias_ref,
        normalizer_ref,
        stabilizer_ref,
        ids_ref,
        route_ref,
        mix_ref,
        query_ref,
        key_ref,
        value_ref,
        gate_ref,
    ) = refs[:16]
    loads_from = refs[16:25]
    out_ref, projected_ref, gates_ref = refs[25:28]
    loaded = refs[28:37]
    (
        normed_buf,
        rows_buf,
        weight_buf,
        product_buf,
        result_buf,
        mix_buf,
        split_buf,
        gated_src,
        gated_buf,
        columns_buf,
        mixed_buf,
        outgoing,
        arrived,
        answer,
        returned,
        load_sems,
        send_sems,
        recv_sems,
    ) = refs[37:]
    weights = loaded[:6]
    input_weight, forget_weight, memory = loaded[6:]
    me = lax.axis_index("ep")
    members = n // groups
    plane, place = me // members, lax.rem(me, members)
    part_width = rows_buf.shape[2]
    columns = weight_buf.shape[2]
    per_matrix = query_ref.shape[1] // columns
    greet(n, me)
    projections = (query_ref, key_ref, value_ref, gate_ref)

    def column(block):
        return pl.ds(pl.multiple_of(lax.rem(block, per_matrix) * columns, LANES), columns)

    for index, ref in enumerate(projections):

        @pl.when(place // per_matrix == index)
        def _():
            pltpu.make_async_copy(
                ref.at[:, column(place)], weight_buf.at[place], recv_sems.at[1]
            ).start()

    pltpu.make_async_copy(mix_ref, mix_buf.at[place], recv_sems.at[3]).start()
    loads = [
        pltpu.make_async_copy(source, target, load_sems.at[index])
        for index, (source, target) in enumerate(zip(loads_from, loaded))
    ]
    residual = tokens_ref[...].astype(jnp.float32)
    normed = rms_scale(residual, premix_ref[...]).astype(jnp.bfloat16)
    for group in range(groups):
        normed_buf[group] = normed[:, group * part_width : (group + 1) * part_width]
    pltpu.make_async_copy(normed_buf.at[plane], rows_buf.at[me], recv_sems.at[0]).start()
    greeted(n)

    def send_rows(i, carry):
        peer = lax.rem(me + i, n)
        send(
            normed_buf.at[peer // members],
            rows_buf.at[me],
            send_sems.at[0],
            recv_sems.at[0],
            peer,
        )
        return carry

    def send_weights(i, carry):
        block = lax.rem(place + i, members)
        for index, ref in enumerate(projections):

            @pl.when(block // per_matrix == index)
            def _():
                send(
                    ref.at[:, column(block)],
                    weight_buf.at[place],
                    send_sems.at[1],
                    recv_sems.at[1],
                    plane * members + block,
                )

        return carry

    lax.fori_loop(1, members, send_weights, 0)
    lax.fori_loop(1, n, send_rows, 0)
    for index in (6, 7, 8, 3, 4, 5, 0, 1, 2):
        loads[index].start()

    loads[6].wait()
    loads[7].wait()
    input_pre = (
        jnp.dot(normed, input_weight[...], preferred_element_type=jnp.float32)
        + input_bias_ref[...]
    )
    forget_pre = (
        jnp.dot(normed, forget_weight[...], preferred_element_type=jnp.float32)
        + forget_bias_ref[...]
    )
    carried = (
        jnp.minimum(forget_pre, 0.0)
        - jnp.log1p(jnp.exp(-jnp.abs(forget_pre)))
        + stabilizer_ref[...]
    )
    next_stabilizer = jnp.maximum(carried, input_pre)
    keep_old = jnp.exp(carried - next_stabilizer)
    write_new = jnp.exp(input_pre - next_stabilizer)
    gates_ref[0] = keep_old
    gates_ref[1] = write_new
    gates_ref[2] = next_stabilizer
    local, capacity, width = outgoing.shape[1:]
    slots, combine = routing(ids_ref[...], route_ref[...], n * local * capacity, capacity)
    dispatch = slots.T.astype(jnp.bfloat16)
    sequences, heads, head_width = memory.shape[:3]
    loads[8].wait()

    def split(s, carry):
        for head in range(heads):
            value = memory[s, head]
            high = value.astype(jnp.bfloat16)
            rows = pl.ds(pl.multiple_of(s * head_width, LANES), head_width)
            split_buf[head, rows, :head_width] = high
            split_buf[head, rows, head_width:] = (value - high.astype(jnp.float32)).astype(
                jnp.bfloat16
            )
        return carry

    lax.fori_loop(0, sequences, split, 0)

    drain(rows_buf, recv_sems.at[0])
    drain(weight_buf, recv_sems.at[1])
    rows = rows_buf[...].reshape(rows_buf.shape[0] * rows_buf.shape[1], part_width)
    weight = weight_buf[...].reshape(weight_buf.shape[0] * weight_buf.shape[1], columns)
    product = jnp.dot(rows, weight, preferred_element_type=jnp.float32)
    product_buf[...] = product.reshape(product_buf.shape).astype(jnp.bfloat16)
    pltpu.make_async_copy(product_buf.at[me], result_buf.at[me], recv_sems.at[2]).start()

    def exchange(source, target, stage):
        def one(i, carry):
            peer = lax.rem(me + i, n)
            send(source.at[peer], target.at[me], send_sems.at[stage], recv_sems.at[stage], peer)
            return carry

        lax.fori_loop(1, n, one, 0)

    def send_mix(i, carry):
        send(
            mix_ref,
            mix_buf.at[place],
            send_sems.at[3],
            recv_sems.at[3],
            plane * members + lax.rem(place + i, members),
        )
        return carry

    def line(source, target, stage):
        for i in range(1, groups):
            peer = lax.rem(plane + i, groups)
            send(
                source(peer),
                target.at[plane],
                send_sems.at[stage],
                recv_sems.at[stage],
                peer * members + place,
            )

    exchange(product_buf, result_buf, 2)
    lax.fori_loop(1, members, send_mix, 0)
    drain(result_buf, recv_sems.at[2])
    for member in range(members):
        total = result_buf[member].astype(jnp.float32)
        for group in range(1, groups):
            total = total + result_buf[group * members + member].astype(jnp.float32)
        total = total.astype(jnp.bfloat16).astype(jnp.float32)
        projected_ref[:, member * columns : (member + 1) * columns] = total
    memory_width = heads * head_width
    row = lax.broadcasted_iota(jnp.int32, (sequences, head_width), 0)
    for head in range(heads):

        def piece(matrix):
            start = matrix * memory_width + head * head_width
            return projected_ref[:, start : start + head_width]

        span = slice(head * head_width, (head + 1) * head_width)
        query, value, out_gate = piece(0), piece(2), piece(3)
        key = piece(1) * head_width ** (-0.5)
        keep, write = keep_old[:, head : head + 1], write_new[:, head : head + 1]
        local_score = write * jnp.sum(query * key, axis=-1, keepdims=True)
        denominator = (
            keep * jnp.sum(normalizer_ref[:, span] * query, axis=-1, keepdims=True) + local_score
        )
        narrow = query.astype(jnp.bfloat16)
        reads = lax.dot_general(
            jnp.concatenate([narrow, narrow], axis=1),
            split_buf[head],
            (((1,), (1,)), ((), ())),
            preferred_element_type=jnp.float32,
        )
        read = jnp.zeros((sequences, head_width), jnp.float32)
        for s in range(sequences):
            read = jnp.where(row == s, reads[:, s * head_width : (s + 1) * head_width], read)
        memory_read = (keep * read + local_score * value) / jnp.maximum(
            jnp.abs(denominator), 1.0
        )
        gated_src[:, span] = (jax.nn.sigmoid(out_gate) * memory_read).astype(jnp.bfloat16)

    pltpu.make_async_copy(gated_src, gated_buf.at[plane], recv_sems.at[4]).start()
    line(lambda peer: gated_src, gated_buf, 4)
    drain(mix_buf, recv_sems.at[3])
    drain(gated_buf, recv_sems.at[4])
    gated = gated_buf[...].reshape(gated_buf.shape[0] * gated_buf.shape[1], gated_buf.shape[2])
    mix_weight = mix_buf[...].reshape(mix_buf.shape[0] * mix_buf.shape[1], mix_buf.shape[2])
    columns_buf[...] = (
        lax.dot_general(
            gated, mix_weight, (((1,), (1,)), ((), ())), preferred_element_type=jnp.float32
        )
        .reshape(columns_buf.shape)
        .astype(jnp.bfloat16)
    )
    pltpu.make_async_copy(columns_buf.at[plane], mixed_buf.at[plane], recv_sems.at[5]).start()
    line(lambda peer: columns_buf.at[peer], mixed_buf, 5)
    drain(mixed_buf, recv_sems.at[5])
    mixed = jnp.concatenate([mixed_buf[group] for group in range(groups)], axis=1)
    after_mix = (residual + rms_scale(mixed.astype(jnp.float32), postmix_ref[...])).astype(
        jnp.bfloat16
    )
    after_float = after_mix.astype(jnp.float32)
    token_rows = rms_scale(after_float, prefeed_ref[...]).astype(jnp.bfloat16)
    outgoing[...] = (
        jnp.dot(dispatch, token_rows, preferred_element_type=jnp.float32)
        .reshape(outgoing.shape)
        .astype(jnp.bfloat16)
    )
    pltpu.make_async_copy(outgoing.at[me], arrived.at[me], recv_sems.at[6]).start()
    exchange(outgoing, arrived, 6)
    for index in (3, 4, 5):
        loads[index].wait()
    shared_out = two_layer(token_rows, weights[3][...], weights[4][...], weights[5][...])
    for index in (0, 1, 2):
        loads[index].wait()
    drain(arrived, recv_sems.at[6])
    for item in range(local):
        block = arrived[:, item].astype(jnp.float32).reshape(n * capacity, width)
        answer[:, item] = (
            two_layer(
                block.astype(jnp.bfloat16),
                weights[0][item],
                weights[1][item],
                weights[2][item],
            )
            .reshape(n, capacity, width)
            .astype(jnp.bfloat16)
        )
    pltpu.make_async_copy(answer.at[me], returned.at[me], recv_sems.at[7]).start()
    exchange(answer, returned, 7)
    high = combine.astype(jnp.bfloat16)
    low = (combine - high.astype(jnp.float32)).astype(jnp.bfloat16)
    drain(returned, recv_sems.at[7])
    picked = (
        returned[...].astype(jnp.float32).reshape(combine.shape[1], width).astype(jnp.bfloat16)
    )
    combined = (
        shared_out
        + jnp.dot(high, picked, preferred_element_type=jnp.float32)
        + jnp.dot(low, picked, preferred_element_type=jnp.float32)
    )
    out_ref[...] = (after_float + rms_scale(combined, postfeed_ref[...])).astype(jnp.bfloat16)
    drain(rows_buf.at[pl.ds(0, n - 1)], send_sems.at[0])
    drain(weight_buf.at[pl.ds(0, members - 1)], send_sems.at[1])
    drain(result_buf.at[pl.ds(0, n - 1)], send_sems.at[2])
    drain(mix_buf.at[pl.ds(0, members - 1)], send_sems.at[3])
    drain(gated_buf.at[pl.ds(0, groups - 1)], send_sems.at[4])
    drain(mixed_buf.at[pl.ds(0, groups - 1)], send_sems.at[5])
    drain(arrived.at[pl.ds(0, n - 1)], send_sems.at[6])
    drain(returned.at[pl.ds(0, n - 1)], send_sems.at[7])


def layer(n, groups, small, projections, loads, capacity):
    tokens, mix_weight = small[0], small[-1]
    sequences, width = tokens.shape
    depth, columns = projections[0].shape
    members = n // groups
    wide = 4 * columns // members
    local = loads[0].shape[0]
    heads, head_width = loads[8].shape[1:3]
    narrow = functools.partial(pltpu.VMEM, dtype=jnp.bfloat16)
    slots = narrow((n, local, capacity, width))
    pieces = narrow((groups, sequences, width // groups))
    return pl.pallas_call(
        functools.partial(layer_kernel, n, groups),
        out_shape=(
            jax.ShapeDtypeStruct((sequences, width), jnp.bfloat16),
            jax.ShapeDtypeStruct((sequences, 4 * columns), jnp.float32),
            jax.ShapeDtypeStruct((3, sequences, heads), jnp.float32),
        ),
        in_specs=[VM] * len(small) + [ANY] * (len(projections) + len(loads)),
        out_specs=(VM, VM, VM),
        scratch_shapes=[pltpu.VMEM(w.shape, w.dtype) for w in loads]
        + [
            pieces,
            narrow((n, sequences, width // groups)),
            narrow((members, depth, wide)),
            narrow((n, sequences, wide)),
            narrow((n, sequences, wide)),
            narrow((members,) + mix_weight.shape),
            narrow((heads, sequences * head_width, 2 * head_width)),
            narrow((sequences, columns)),
            narrow((groups, sequences, columns)),
            pieces,
            pieces,
        ]
        + [slots] * 4
        + [
            pltpu.SemaphoreType.DMA((len(loads),)),
            pltpu.SemaphoreType.DMA((8,)),
            pltpu.SemaphoreType.DMA((8,)),
        ],
        compiler_params=pltpu.CompilerParams(
            collective_id=0, has_side_effects=True, vmem_limit_bytes=56 * 1024 * 1024
        ),
    )(*small, *projections, *loads)


def on_device(
    tokens,
    premix_gain,
    postmix_gain,
    prefeed_gain,
    postfeed_gain,
    query_weight,
    key_weight,
    value_weight,
    outgate_weight,
    ingate_weight,
    forget_weight,
    ingate_bias,
    forget_bias,
    memory_state,
    normalizer,
    stabilizer,
    output_weight,
    expert_ids,
    route_weights,
    expert_gate,
    expert_up,
    expert_down,
    shared_gate,
    shared_up,
    shared_down,
):
    sequences = tokens.shape[0]
    memory_width = query_weight.shape[1]
    heads, head_width = memory_state.shape[1:3]
    devices = lax.axis_size("ep")
    experts_total = expert_gate.shape[0] * devices
    choose_count = expert_ids.shape[1]
    capacity = min(
        sequences, max(2, 2 * ((sequences * choose_count + experts_total - 1) // experts_total))
    )
    next_tokens, projected, gates = layer(
        devices,
        GROUPS,
        (
            tokens,
            premix_gain[None],
            postmix_gain[None],
            prefeed_gain[None],
            postfeed_gain[None],
            ingate_bias[None],
            forget_bias[None],
            normalizer.reshape(sequences, memory_width),
            stabilizer,
            expert_ids,
            route_weights,
            output_weight.T,
        ),
        (query_weight, key_weight, value_weight, outgate_weight),
        (
            expert_gate,
            expert_up,
            expert_down,
            shared_gate,
            shared_up,
            shared_down,
            ingate_weight,
            forget_weight,
            memory_state,
        ),
        capacity,
    )
    keep_old, write_new, next_stabilizer = gates[0], gates[1], gates[2]
    split = projected.reshape(sequences, 4, heads, head_width)
    key_heads = split[:, 1] * head_width ** (-0.5)
    value_heads = split[:, 2]
    next_memory = (
        keep_old[..., None, None] * memory_state
        + write_new[..., None, None] * value_heads[..., :, None] * key_heads[..., None, :]
    )
    next_normalizer = keep_old[..., None] * normalizer + write_new[..., None] * key_heads
    return (next_tokens, next_memory, next_normalizer, next_stabilizer)


def solution(mesh):
    in_specs = (
        P("ep", None),
        P(),
        P(),
        P(),
        P(),
        P("ep", None),
        P("ep", None),
        P("ep", None),
        P("ep", None),
        P(),
        P(),
        P(),
        P(),
        P("ep", None, None, None),
        P("ep", None, None),
        P("ep", None),
        P(None, "ep"),
        P("ep", None),
        P("ep", None),
        P("ep", None, None),
        P("ep", None, None),
        P("ep", None, None),
        P(),
        P(),
        P(),
    )
    out_specs = (P("ep", None), P("ep", None, None, None), P("ep", None, None), P("ep", None))
    return jax.shard_map(
        on_device, mesh=mesh, in_specs=in_specs, out_specs=out_specs, check_vma=False
    )
```

time: 196 us -> 80 us (0.41)
  the two profiles are of different devices: /device:TPU:0 before, /device:TPU:29 now
where the time goes in v3:
time: 80 us; the launch traced here: 79.4 us
  Pallas kernels  64.5 us (81%)
  local copies, waits for them, and re-layouts  7.65 us (10%)
  other arithmetic  6.59 us (8%)
    pallas_call x1, Pallas kernels, layer(): pl.pallas_call(functools.partial(layer_kernel, n, groups), out_shape=(jax...  64.5 us
    unnamed x8, local copies, waits for them, and re-layouts  5.53 us
    add x1, other arithmetic, on_device(): keep_old[..., None, None] * memory_state  4.37 us

profile of v3, /device:TPU:29, one launch (start us, length us, event | category | flops | bytes accessed | tf_op | source)
XLA Modules:
  0.0 79.4 jit_solution(12328380522851550207)
XLA Ops:
  0.6 1.4 %copy.42 = f32[1,8,8,128]{3,1,2,0:T(8,128)} copy(f32[1,8,8,128]{3,2,1,0:T(8,128)} %bitcast.32) | data formatting | bytes 65536
  2.0 1.8 %copy.29.refs_22_ = bf16[2048,8]{1,0:T(8,128)(2,1)} copy(bf16[2048,8]{0,1:T(8,128)(2,1)} %param.34) | data formatting | bytes 65536 | tf_op args[9]
  3.8 1.8 %copy.30.refs_23_ = bf16[2048,8]{1,0:T(8,128)(2,1)} copy(bf16[2048,8]{0,1:T(8,128)(2,1)} %param.35) | data formatting | bytes 65536 | tf_op args[10]
  5.5 0.0 copy-start
  5.5 64.5 %shard_map.264 = (bf16[8,2048]{1,0:T(8,128)(2,1)}, f32[8,4096]{1,0:T(8,128)}, f32[3,8,8]{2,1,0:T(8,128)}) custom-call(bf16[8,2048]{1,0:T(8,128)(2,1)} %refs_0_.1, f32[1,2048]{1,0:T(1,128)} %bitcast.35, f32[1,2048]{1,0:T(1,128)} %bitcast.36, f32[1,2048]{1,0:T(1,128)} %bitcast.37, f32[1,2048]{1,0:T(1,128)} %bitcast.38, f32[1,8]{1,0:T(1,128)} %bitcast.39, ...), custom_call_target="tpu_custom_call" | custom-call | tf_op jit(solution)/shard_map/pallas_call | solution.py:389
  70.1 0.7 broadcast_multiply_fusion
  70.8 1.3 %slice_bitcast_fusion.1 = (f32[8,8]{1,0:T(8,128)}, f32[8,8]{1,0:T(8,128)S(1)}, f32[8,8]{1,0:T(8,128)S(1)}) fusion(f32[3,8,8]{2,1,0:T(8,128)} %get-tuple-element.8), kind=kLoop, calls=%fused_computation.7 | loop fusion | bytes 1536 | tf_op jit(solution)/shard_map/squeeze | solution.py:491
  72.0 0.1 copy.31
  72.1 0.8 %fusion = f32[8,8,128]{2,0,1:T(8,128)S(1)} fusion(f32[8,4,8,128]{3,0,2,1:T(8,128)} %bitcast.33, f32[8,8]{0,1:T(8,128)S(1)} %copy.31), kind=kLoop, calls=%fused_computation.3 | loop fusion | flops 8192 | bytes 65792 | tf_op jit(solution)/shard_map/mul | solution.py:497
  72.9 0.8 slice.21
  73.7 0.0 copy-done
  73.7 0.7 multiply_add_fusion.1
  74.4 0.0 copy-start.1
  74.4 4.4 %multiply_add_fusion = f32[8,8,128,128]{3,2,1,0:T(8,128)} fusion(f32[8,8,128,128]{3,2,1,0:T(8,128)} %refs_24_.1, f32[8,8,128]{2,1,0:T(8,128)S(1)} %get-tuple-element.11, f32[8,8,128]{2,1,0:T(8,128)S(1)} %copy.32, f32[8,8]{1,0:T(8,128)S(1)} %get-tuple-element.14), kind=kLoop, calls=%fused_computation | loop fusion | flops 3145728 | bytes 8454400 | tf_op jit(solution)/shard_map/add | solution.py:496
  78.8 0.0 copy-done.1
  78.8 0.6 copy.44
  (1 shorter events, 0.0 us)
Async XLA Ops:
  5.5 68.2 %copy-start = (f32[8,8,128]{2,1,0:T(8,128)S(1)}, f32[8,8,128]{2,1,0:T(8,128)}, u32[]{:S(2)}) copy-start(f32[8,8,128]{2,1,0:T(8,128)} %param.39) | copy-start | bytes 98308
  74.4 4.4 %copy-start.1 = (bf16[8,2048]{1,0:T(8,128)(2,1)S(1)}, bf16[8,2048]{1,0:T(8,128)(2,1)}, u32[]{:S(2)}) copy-start(bf16[8,2048]{1,0:T(8,128)(2,1)} %get-tuple-element.19) | copy-start | bytes 98308

commit v4 on v3

--- a/solution.py
+++ b/solution.py
@@ -70,6 +70,12 @@
         earlier = earlier + jnp.where(row > other, chosen[other : other + 1], 0.0)
     slots = jnp.where(earlier == turn, chosen, 0.0)
     return slots, slots * weight_of
+
+
+def across(left, right):
+    return lax.dot_general(
+        left, right, (((1,), (1,)), ((), ())), preferred_element_type=jnp.float32
+    )
 
 
 def two_layer(rows, gate_weight, up_weight, down_weight):
@@ -190,11 +196,11 @@
     loads[6].wait()
     loads[7].wait()
     input_pre = (
-        jnp.dot(normed, input_weight[...], preferred_element_type=jnp.float32)
+        across(normed, input_weight[...])
         + input_bias_ref[...]
     )
     forget_pre = (
-        jnp.dot(normed, forget_weight[...], preferred_element_type=jnp.float32)
+        across(normed, forget_weight[...])
         + forget_bias_ref[...]
     )
     carried = (
@@ -287,7 +293,7 @@
         keep, write = keep_old[:, head : head + 1], write_new[:, head : head + 1]
         local_score = write * jnp.sum(query * key, axis=-1, keepdims=True)
         denominator = (
-            keep * jnp.sum(normalizer_ref[:, span] * query, axis=-1, keepdims=True) + local_score
+            keep * jnp.sum(normalizer_ref[:, head, :] * query, axis=-1, keepdims=True) + local_score
         )
         narrow = query.astype(jnp.bfloat16)
         reads = lax.dot_general(
@@ -421,6 +427,80 @@
     )(*small, *projections, *loads)
 
 
+def state_kernel(
+    tokens_ref,
+    projected_ref,
+    gates_ref,
+    normalizer_ref,
+    memory_ref,
+    next_tokens_ref,
+    next_memory_ref,
+    next_normalizer_ref,
+    next_stabilizer_ref,
+):
+    step = pl.program_id(0)
+    block, heads, head_width = memory_ref.shape[:3]
+    memory_width = heads * head_width
+    scale = head_width ** (-0.5)
+
+    @pl.when(step == 0)
+    def _():
+        next_tokens_ref[...] = tokens_ref[...]
+        next_stabilizer_ref[...] = gates_ref[2]
+        keep_all, write_all = gates_ref[0], gates_ref[1]
+        for head in range(heads):
+            start = memory_width + head * head_width
+            next_normalizer_ref[:, head, :] = keep_all[:, head : head + 1] * normalizer_ref[
+                :, head, :
+            ] + write_all[:, head : head + 1] * (
+                projected_ref[:, start : start + head_width] * scale
+            )
+
+    for item in range(block):
+        row = pl.ds(step * block + item, 1)
+        keep, write = gates_ref[0, row, :], gates_ref[1, row, :]
+        keys = projected_ref[row, memory_width : 2 * memory_width] * scale
+        values = projected_ref[row, 2 * memory_width : 3 * memory_width]
+        stacked = jnp.concatenate(
+            [
+                write[:, head : head + 1] * values[:, head * head_width : (head + 1) * head_width]
+                for head in range(heads)
+            ],
+            axis=0,
+        ).T
+        for head in range(heads):
+            next_memory_ref[item, head] = (
+                keep[:, head : head + 1] * memory_ref[item, head]
+                + stacked[:, head : head + 1]
+                * keys[:, head * head_width : (head + 1) * head_width]
+            )
+
+
+def write_state(tokens, projected, gates, normalizer, memory):
+    sequences = memory.shape[0]
+    steps = 4
+    block = (sequences // steps,) + memory.shape[1:]
+
+    def whole(array):
+        return pl.BlockSpec(array.shape, lambda i, rank=array.ndim: (0,) * rank)
+
+    moving = pl.BlockSpec(block, lambda i: (i, 0, 0, 0))
+    stabilizer = jax.ShapeDtypeStruct(gates.shape[1:], jnp.float32)
+    return pl.pallas_call(
+        state_kernel,
+        grid=(steps,),
+        out_shape=(
+            jax.ShapeDtypeStruct(tokens.shape, tokens.dtype),
+            jax.ShapeDtypeStruct(memory.shape, memory.dtype),
+            jax.ShapeDtypeStruct(normalizer.shape, normalizer.dtype),
+            stabilizer,
+        ),
+        in_specs=[whole(tokens), whole(projected), whole(gates), whole(normalizer), moving],
+        out_specs=(whole(tokens), moving, whole(normalizer), whole(stabilizer)),
+        compiler_params=pltpu.CompilerParams(dimension_semantics=("arbitrary",)),
+    )(tokens, projected, gates, normalizer, memory)
+
+
 def on_device(
     tokens,
     premix_gain,
@@ -449,8 +529,6 @@
     shared_down,
 ):
     sequences = tokens.shape[0]
-    memory_width = query_weight.shape[1]
-    heads, head_width = memory_state.shape[1:3]
     devices = lax.axis_size("ep")
     experts_total = expert_gate.shape[0] * devices
     choose_count = expert_ids.shape[1]
@@ -468,7 +546,7 @@
             postfeed_gain[None],
             ingate_bias[None],
             forget_bias[None],
-            normalizer.reshape(sequences, memory_width),
+            normalizer,
             stabilizer,
             expert_ids,
             route_weights,
@@ -482,22 +560,13 @@
             shared_gate,
             shared_up,
             shared_down,
-            ingate_weight,
-            forget_weight,
+            ingate_weight.T,
+            forget_weight.T,
             memory_state,
         ),
         capacity,
     )
-    keep_old, write_new, next_stabilizer = gates[0], gates[1], gates[2]
-    split = projected.reshape(sequences, 4, heads, head_width)
-    key_heads = split[:, 1] * head_width ** (-0.5)
-    value_heads = split[:, 2]
-    next_memory = (
-        keep_old[..., None, None] * memory_state
-        + write_new[..., None, None] * value_heads[..., :, None] * key_heads[..., None, :]
-    )
-    next_normalizer = keep_old[..., None] * normalizer + write_new[..., None] * key_heads
-    return (next_tokens, next_memory, next_normalizer, next_stabilizer)
+    return write_state(next_tokens, projected, gates, normalizer, memory_state)
 
 
 def solution(mesh):

time: 80 us -> 72.1 us (0.901)
  local copies, waits for them, and re-layouts: 7.65 us -> 0 us
  Pallas kernels: 64.5 us -> 71.2 us
  other arithmetic: 6.59 us -> 0 us
    pallas_call x0 -> x1, Pallas kernels: none -> 6.65 us  [write_state(): pl.pallas_call(state_kernel, grid=(steps,), out_shape=(jax.ShapeDtypeStru...]
    unnamed x8 -> x0, local copies, waits for them, and re-layouts: 5.53 us -> none
    add x2 -> x0, other arithmetic: 5.07 us -> none  [the longest x1 4.37 us: on_device(): keep_old[..., None, None] * memory_state]
    mul x2 -> x0, other arithmetic: 1.52 us -> none  [the longest x1 0.83 us: on_device(): write_new[..., None, None] * value_heads[..., :, None]]
    squeeze x1 -> x0, local copies, waits for them, and re-layouts: 1.28 us -> none  [on_device(): keep_old, write_new, next_stabilizer = (gates[0], gates[1], gates[2])]
where the time goes in v4:
time: 72.1 us; the launch traced here: 71.8 us
  Pallas kernels  71.2 us (99%)
    pallas_call x1, Pallas kernels, layer(): pl.pallas_call(functools.partial(layer_kernel, n, groups), out_shape=(jax...  64.5 us
    pallas_call x1, Pallas kernels, write_state(): pl.pallas_call(state_kernel, grid=(steps,), out_shape=(jax.ShapeDtypeStru...  6.65 us

profile of v4, /device:TPU:29, one launch (start us, length us, event | category | flops | bytes accessed | tf_op | source)
XLA Modules:
  0.0 71.8 jit_solution(10846911405873004690)
XLA Ops:
  0.6 64.5 %shard_map.264 = (bf16[8,2048]{1,0:T(8,128)(2,1)}, f32[8,4096]{1,0:T(8,128)}, f32[3,8,8]{2,1,0:T(8,128)}) custom-call(bf16[8,2048]{1,0:T(8,128)(2,1)} %refs_0_.1, f32[1,2048]{1,0:T(1,128)} %bitcast.12, f32[1,2048]{1,0:T(1,128)} %bitcast.13, f32[1,2048]{1,0:T(1,128)} %bitcast.14, f32[1,2048]{1,0:T(1,128)} %bitcast.15, f32[1,8]{1,0:T(1,128)} %bitcast.16, ...), custom_call_target="tpu_custom_call" | custom-call | tf_op jit(solution)/shard_map/pallas_call | solution.py:395
  65.2 6.7 %shard_map.265 = (bf16[8,2048]{1,0:T(8,128)(2,1)}, f32[8,8,128,128]{3,2,1,0:T(8,128)}, f32[8,8,128]{2,1,0:T(8,128)}, f32[8,8]{1,0:T(8,128)}) custom-call(bf16[8,2048]{1,0:T(8,128)(2,1)} %get-tuple-element.7.tokens_ref, f32[8,4096]{1,0:T(8,128)} %get-tuple-element.8.projected_ref, f32[3,8,8]{2,1,0:T(8,128)} %get-tuple-element.9.gates_ref, ...), custom_call_target="tpu_custom_call" | custom-call | tf_op jit(solution)/shard_map/pallas_call | solution.py:489
